TPU v7x, 256 devices: a 2x2x32 block of a 4x16x32 slice. The times are simulated.
256 devices in a mesh: grp: 4 (over y, x), sp: 32 (over z), tp: 2 (over core).
Axes of the slice: x: 2, y: 2, z: 32, core: 2. Of those that a mesh axis runs over, the one named last changes fastest.
The devices are a block of a 4x16x32 slice.
Arguments:
- tokens: bfloat16 [65536, 2048], P(('grp', 'sp', 'tp')), parts along dimension 0, may hold values from -60 to 60
- query_weight: bfloat16 [2048, 1024], P(None, 'tp'), may hold values from -0.125 to 0.125
- key_weight: bfloat16 [2048, 1024], P(None, 'tp'), may hold values from -0.125 to 0.125
- value_weight: bfloat16 [2048, 1024], P(None, 'tp'), may hold values from -0.125 to 0.125
- output_weight: bfloat16 [1024, 2048], P(None, 'tp'), may hold values from -1.5 to 1.5
Outputs:
- attended: bfloat16 [65536, 2048], P(('grp', 'sp'), 'tp'), parts along dimension 0
There are 4 independent parts, one for each index of `grp`. A program takes and returns all parts, laid end to end along the dimension named above; an argument that names none is the same for every part. Nothing has to cross between parts.
All inputs are finite; a program needn't handle non-finite values.
Results may differ from a plain program's by a relative error of at most 0.012.
The roundings to bfloat16 on the way count: a program that leaves them out, or rounds other values in their place, can miss the bound.
Values may be sent and summed in bfloat16 or wider, within the bound.
A program may use at most 128 MiB of HBM per device.

v0:
```python
import jax
import jax.numpy as jnp
from jax import lax
from jax.sharding import PartitionSpec as P

HEAD = 128
REACH_STEPS = 128
MIDDLE_DILATION = 4
FAR_DILATION = 16


THETA_BASE = 500000.0


def laid_out(pieces, dim):
    pieces = jnp.moveaxis(pieces, 0, dim)
    lengths = pieces.shape
    return pieces.reshape(*lengths[:dim], lengths[dim] * lengths[dim + 1], *lengths[dim + 2 :])


def sent_to_all(shard, axis):
    copies = jnp.broadcast_to(shard, (lax.axis_size(axis), *shard.shape))
    return lax.all_to_all(copies, axis, split_axis=0, concat_axis=0, tiled=True)


def gathered_copies(shard, axis, dim):
    return laid_out(sent_to_all(shard, axis), dim)


def passed_along(block, axis, distance):
    devices = range(lax.axis_size(axis))
    route = [(i - distance, i) for i in devices if i - distance in devices]
    return lax.ppermute(block, axis, route)


def rotate(values, positions):
    half = values.shape[-1] // 2
    inverse = THETA_BASE ** (-jnp.arange(half, dtype=jnp.float32) / half)
    angles = positions[:, None, None] * inverse
    cosine = jnp.cos(angles)
    sine = jnp.sin(angles)
    first = values[..., :half]
    second = values[..., half:]
    return jnp.concatenate(
        [first * cosine - second * sine, second * cosine + first * sine], axis=-1
    )


def windowed(queries, key_context, value_context, pattern_dilation, context_start):
    query_rows, heads, size = queries.shape
    sub_length = query_rows // pattern_dilation
    if sub_length >= REACH_STEPS:
        blocks = sub_length // REACH_STEPS
        block_rows = REACH_STEPS
        query_blocks = queries.reshape(blocks, REACH_STEPS, pattern_dilation, heads, size)

        def arrange(array):
            whole = array.reshape(blocks + 1, REACH_STEPS, pattern_dilation, heads, size)
            return jnp.concatenate([whole[:-1], whole[1:]], axis=1)

    else:
        blocks = 1
        block_rows = sub_length
        query_blocks = queries.reshape(1, sub_length, pattern_dilation, heads, size)

        def arrange(array):
            return array.reshape(1, sub_length + REACH_STEPS, pattern_dilation, heads, size)

    key_blocks = arrange(key_context)
    value_blocks = arrange(value_context)
    scores = jnp.einsum(
        "nqrhd,nkrhd->nrhqk", query_blocks, key_blocks, preferred_element_type=jnp.float32
    ) * HEAD ** (-0.5)
    query_index = jnp.arange(block_rows)[:, None] + REACH_STEPS
    key_index = jnp.arange(block_rows + REACH_STEPS)[None, :]
    distance = query_index - key_index
    sub_index = (
        jnp.arange(blocks)[:, None] * block_rows + jnp.arange(block_rows + REACH_STEPS)[None, :]
    )
    key_position = (
        context_start
        + sub_index[:, None, :] * pattern_dilation
        + jnp.arange(pattern_dilation)[None, :, None]
    )
    allowed = ((distance >= 0) & (distance <= REACH_STEPS))[None, None, None] & (key_position >= 0)[
        :, :, None, None, :
    ]
    scores = jnp.where(allowed, scores, -jnp.inf)
    top = jnp.max(scores, axis=-1, keepdims=True)
    offset_keys = jnp.exp(scores - top)
    total = jnp.sum(offset_keys, axis=-1, keepdims=True)
    weights = (offset_keys / total).astype(jnp.bfloat16)
    result = jnp.einsum(
        "nrhqk,nkrhd->nqrhd", weights, value_blocks, preferred_element_type=jnp.float32
    ).reshape(query_rows, heads, size)
    lse = jnp.transpose((top + jnp.log(total))[..., 0], (0, 3, 1, 2)).reshape(query_rows, heads)
    return (result, lse)


def body(tokens, query_weight, key_weight, value_weight, output_weight):
    width = query_weight.shape[1]
    heads = width // HEAD
    piece = gathered_copies(tokens, "tp", 0)
    projected = jnp.stack(
        [
            jnp.dot(piece, query_weight, preferred_element_type=jnp.float32),
            jnp.dot(piece, key_weight, preferred_element_type=jnp.float32),
            jnp.dot(piece, value_weight, preferred_element_type=jnp.float32),
        ]
    )
    query_rows = projected.shape[1]
    offset = lax.axis_index("sp") * query_rows
    positions = (offset + jnp.arange(query_rows, dtype=jnp.int32)).astype(jnp.float32)
    queries = rotate(projected[0].reshape(query_rows, heads, HEAD), positions).astype(jnp.bfloat16)
    keys = rotate(projected[1].reshape(query_rows, heads, HEAD), positions).astype(jnp.bfloat16)
    values = projected[2].astype(jnp.bfloat16).reshape(query_rows, heads, HEAD)
    matched_pairs = jnp.stack([keys, values])
    reach_extent = -(-(FAR_DILATION * REACH_STEPS) // query_rows)
    context = matched_pairs
    holding = 1
    while holding < reach_extent + 1:
        count = min(holding, reach_extent + 1 - holding)
        newest = context[:, context.shape[1] - count * query_rows :]
        received = passed_along(newest, "sp", holding)
        context = jnp.concatenate([received, context], axis=1)
        holding = holding + count
    context_length = context.shape[1]
    results = []
    lses = []
    for pattern_dilation in (1, MIDDLE_DILATION, FAR_DILATION):
        reach_rows = pattern_dilation * REACH_STEPS
        window = context[:, context_length - query_rows - reach_rows :]
        result, lse = windowed(queries, window[0], window[1], pattern_dilation, offset - reach_rows)
        results.append(result)
        lses.append(lse)
    mixing = jax.nn.softmax(jnp.stack(lses, axis=0), axis=0)
    mixed = jnp.sum(mixing[..., None] * jnp.stack(results, axis=0), axis=0)
    mixed = mixed.astype(jnp.bfloat16).reshape(query_rows, width)
    attended = jnp.dot(
        gathered_copies(mixed, "tp", 1), output_weight, preferred_element_type=jnp.float32
    )
    return attended.astype(jnp.bfloat16)


def solution(mesh):
    in_specs = (
        P(("grp", "sp", "tp"), None),
        P(None, "tp"),
        P(None, "tp"),
        P(None, "tp"),
        P(None, "tp"),
    )
    out_specs = P(("grp", "sp"), "tp")
    return jax.shard_map(body, mesh=mesh, in_specs=in_specs, out_specs=out_specs, check_vma=False)
```

profile of v0, /device:TPU:2597, one launch (start us, length us, event | category | flops | bytes accessed | tf_op | source)
XLA Modules:
  0.0 275.9 jit_solution(11639673393570624015)
XLA Ops:
  0.0 3.0 %broadcast_in_dim.35 = bf16[2,256,2048]{2,1,0:T(8,128)(2,1)} broadcast(bf16[256,2048]{1,0:T(8,128)(2,1)} %param.5), dimensions={1,2} | broadcast | bytes 3145728 | tf_op jit(solution)/shard_map/broadcast_in_dim | solution.py:22
  3.0 5.4 %all-to-all-start = ((bf16[2,256,2048]{2,1,0:T(8,128)(2,1)}), bf16[2,256,2048]{2,1,0:T(8,128)(2,1)}, u32[]{:S(2)}, u32[]{:S(2)}) async-start(bf16[2,256,2048]{2,1,0:T(8,128)(2,1)} %broadcast_in_dim.35), calls=%async_computation | async-start | bytes 4194304 | tf_op jit(solution)/shard_map/all_to_all | solution.py:23
  8.4 4.0 %copy.141 = bf16[512,2048]{1,0:T(8,128)(2,1)} copy(bf16[512,2048]{0,1:T(8,128)(2,1)} %bitcast.136) | data formatting | bytes 4194304 | tf_op jit(solution)/shard_map/dot_general | solution.py:106
  12.4 4.0 %copy.142 = bf16[512,2048]{1,0:T(8,128)(2,1)} copy(bf16[512,2048]{0,1:T(8,128)(2,1)} %bitcast.137) | data formatting | bytes 4194304 | tf_op jit(solution)/shard_map/dot_general | solution.py:107
  16.3 3.7 %fusion.68 = f32[512,4,128]{0,2,1:T(8,128)S(1)} fusion(bf16[512,2048,1]{1,0,2:T(8,128)(2,1)} %bitcast.1, bf16[4,128,2048]{2,1,0:T(8,128)(2,1)} %bitcast.138), kind=kOutput, calls=%fused_computation.114 | convolution fusion | flops 1073741824 | bytes 5242880 | tf_op jit(solution)/shard_map/dot_general | solution.py:106
  20.0 3.0 %fusion.69 = f32[512,4,128]{0,2,1:T(8,128)S(1)} fusion(bf16[512,2048,1]{1,0,2:T(8,128)(2,1)} %bitcast.1, bf16[4,128,2048]{2,1,0:T(8,128)(2,1)S(1)} %bitcast.139), kind=kOutput, calls=%fused_computation.115 | convolution fusion | flops 1073741824 | bytes 5242880 | tf_op jit(solution)/shard_map/dot_general | solution.py:107
  23.0 2.9 %convolution_convert_fusion.1 = bf16[512,512]{0,1:T(8,128)(2,1)S(1)} fusion(bf16[512,2048]{1,0:T(8,128)(2,1)} %bitcast, bf16[2048,512]{1,0:T(8,128)(2,1)S(1)} %copy-done.23), kind=kOutput, calls=%fused_computation.27 | convolution fusion | flops 1074003968 | bytes 4718592 | tf_op jit(solution)/shard_map/dot_general | solution.py:108
  26.5 1.1 subtract_convert_fusion.1
  27.6 1.0 pad_maximum_fusion
  28.6 2.9 %collective-permute-start = (bf16[2,512,4,128]{1,3,2,0:T(8,128)(2,1)}, bf16[2,512,4,128]{1,3,2,0:T(8,128)(2,1)}, u32[]{:S(2)}, u32[]{:S(2)}) collective-permute-start(bf16[2,512,4,128]{1,3,2,0:T(8,128)(2,1)} %pad_maximum_fusion), channel_id=1, source_target_pairs={{0,2},{2,4},{4,6},{6,8},{8,10},{10,12},{12,14},{14,16},{16,18},{18... | collective-permute-start | bytes 3145736 | tf_op jit(solution)/shard_map/ppermute | solution.py:33
  31.5 4.9 %collective-permute-start.1 = (bf16[2,512,4,128]{1,3,2,0:T(8,128)(2,1)}, bf16[2,512,4,128]{1,3,2,0:T(8,128)(2,1)}, u32[]{:S(2)}, u32[]{:S(2)}) collective-permute-start(bf16[2,512,4,128]{1,3,2,0:T(8,128)(2,1)} %pad_maximum_fusion), channel_id=1, source_target_pairs={{0,8},{2,10},{4,12},{6,14},{8,16},{10,18},{12,20},{14,22},{16,24},... | collective-permute-start | bytes 3145736 | tf_op jit(solution)/shard_map/ppermute | solution.py:33
  36.5 1.0 copy.133
  37.5 1.0 copy.115
  38.5 1.0 copy.114
  41.1 1.9 copy.110
  43.0 1.7 concatenate.91
  44.7 1.0 copy.109
  46.5 0.9 slice.86
  47.4 2.0 copy.123
  49.4 2.0 copy.122
  51.4 2.0 slice.89
  53.4 2.1 copy.135
  55.5 1.9 copy.117
  57.4 0.9 copy.116
  58.4 0.9 copy.112
  59.3 0.9 copy.111
  60.2 2.0 copy.107
  62.2 1.1 copy.106
  63.2 2.0 copy.104
  65.2 2.0 copy.103
  67.2 2.1 copy.130
  69.8 2.9 %maximum_maximum_fusion.1 = bf16[2,1024,4,128]{1,3,2,0:T(8,128)(2,1)} fusion(bf16[1,512,4,128]{1,3,2,0:T(8,128)(2,1)S(1)} %bitcast.117, bf16[1,512,4,64]{1,3,2,0:T(8,128)(2,1)S(1)} %bitcast.121, bf16[1,512,4,64]{1,3,2,0:T(8,128)(2,1)S(1)} %bitcast.124, bf16[2,512,4,128]{1,3,2,0:T(8,128)(2,1)} %collective-permute-done), kind=kLoop, calls=%fused_computation.7 | loop fusion | flops 8388608 | bytes 4194304 | tf_op jit(solution)/shard_map/concatenate | solution.py:125
  72.7 3.7 %collective-permute-start.2 = (bf16[2,1024,4,128]{1,3,2,0:T(8,128)(2,1)}, bf16[2,1024,4,128]{1,3,2,0:T(8,128)(2,1)}, u32[]{:S(2)}, u32[]{:S(2)}) collective-permute-start(bf16[2,1024,4,128]{1,3,2,0:T(8,128)(2,1)} %maximum_maximum_fusion.1), channel_id=1, source_target_pairs={{0,4},{2,6},{4,8},{6,10},{8,12},{10,14},{12,16},{14,18},{16,20},{1... | collective-permute-start | bytes 6291464 | tf_op jit(solution)/shard_map/ppermute | solution.py:33
  76.4 2.3 fusion.67
  78.6 2.0 copy.113
  80.7 1.1 copy.118
  81.8 4.3 %fusion.6 = (f32[4,4,128]{2,1,0:T(4,128)}, f32[4,4,128,256]{3,2,1,0:T(8,128)}) fusion(pred[4,128,256]{2,1,0:T(8,128)(4,1)S(1)} %get-tuple-element.18, bf16[1,128,4,4,64]{4,1,3,2,0:T(8,128)(2,1)} %copy.117, bf16[1,128,4,4,64]{4,1,3,2,0:T(8,128)(2,1)} %copy.116, bf16[1,128,4,4,128]{4,1,3,2,0:T(8,128)(2,1)S(1)} %copy.118, bf16[128,4,4,64]{3,0,2,1:T(8,128)(2,1)} %copy.112, ...), kind=kOutput, calls=%fused_computation.18 | convolution fusion | flops 139982848 | bytes 3809280 | tf_op jit(solution)/shard_map/nqrhd,nkrhd->nrhqk/dot_general | solution.py:71
  86.2 2.3 fusion.66
  88.4 2.0 slice.80
  90.4 2.2 copy.108
  92.5 2.8 %fusion.5 = (f32[4,4,128]{2,1,0:T(4,128)S(1)}, f32[4,4,128,256]{3,2,1,0:T(8,128)S(1)}) fusion(pred[4,128,256]{2,1,0:T(8,128)(4,1)S(1)} %get-tuple-element.17, bf16[4,128,1,4,64]{4,1,3,0,2:T(8,128)(2,1)} %copy.107, bf16[4,128,1,4,64]{4,1,3,0,2:T(8,128)(2,1)} %copy.106, bf16[4,128,1,4,128]{4,1,3,0,2:T(8,128)(2,1)} %copy.108, ...), kind=kOutput, calls=%fused_computation.17 | convolution fusion | flops 139982848 | bytes 3809280 | tf_op jit(solution)/shard_map/nqrhd,nkrhd->nrhqk/dot_general | solution.py:71
  95.4 1.6 fusion.8
  100.6 2.1 copy.132
  102.7 1.1 copy.134
  103.9 2.4 convolution_bitcast_fusion
  106.3 1.7 copy.136
  108.0 2.0 slice.85
  109.9 2.1 copy.129
  112.0 2.6 convolution_bitcast_fusion.1
  114.6 1.1 copy.131
  115.7 120.1 %collective-permute-done.2 = bf16[2,1024,4,128]{1,3,2,0:T(8,128)(2,1)} collective-permute-done((bf16[2,1024,4,128]{1,3,2,0:T(8,128)(2,1)}, bf16[2,1024,4,128]{1,3,2,0:T(8,128)(2,1)}, u32[]{:S(2)}, u32[]{:S(2)}) %collective-permute-start.2) | collective-permute-done | bytes 2097184 | tf_op jit(solution)/shard_map/ppermute | solution.py:33
  235.8 3.0 %maximum_maximum_fusion = bf16[2,2560,4,128]{1,3,2,0:T(8,128)(2,1)S(1)} fusion(bf16[1,512,4,128]{1,3,2,0:T(8,128)(2,1)S(1)} %bitcast.118, bf16[1,512,4,64]{1,3,2,0:T(8,128)(2,1)S(1)} %bitcast.122, bf16[1,512,4,64]{1,3,2,0:T(8,128)(2,1)S(1)} %bitcast.125, bf16[2,512,4,128]{1,3,2,0:T(8,128)(2,1)} %collective-permute-done, ...), kind=kLoop, calls=%fused_computation | loop fusion | flops 31457280 | bytes 10485760 | tf_op jit(solution)/shard_map/concatenate | solution.py:125
  238.8 2.7 fusion.65
  241.5 4.5 %copy.124 = bf16[1,2560,4,128]{3,1,2,0:T(8,128)(2,1)} copy(bf16[1,2560,4,128]{1,3,2,0:T(8,128)(2,1)} %get-tuple-element.5) | data formatting | bytes 5242880 | tf_op jit(solution)/shard_map/slice | solution.py:133
  246.0 3.7 %fusion.7 = (f32[16,4,32]{2,1,0:T(4,128)S(1)}, f32[16,4,32,160]{3,2,1,0:T(8,128)S(1)}) fusion(pred[16,32,160]{2,1,0:T(8,128)(4,1)S(1)} %broadcast_and_fusion, bf16[160,16,4,128]{3,1,0,2:T(8,128)(2,1)} %bitcast.119, bf16[32,16,4,64]{3,0,2,1:T(8,128)(2,1)S(1)} %copy-done.6, bf16[32,16,4,64]{3,0,2,1:T(8,128)(2,1)S(1)} %copy-done.7), kind=kOutput, calls=%fused_computation.19 | convolution fusion | flops 85915648 | bytes 4546560 | tf_op jit(solution)/shard_map/nqrhd,nkrhd->nrhqk/dot_general | solution.py:71
  249.7 1.3 copy-done.1
  251.1 1.0 fusion.10
  252.4 4.4 %copy.137 = bf16[1,2560,4,128]{3,1,2,0:T(8,128)(2,1)} copy(bf16[1,2560,4,128]{1,3,2,0:T(8,128)(2,1)} %get-tuple-element.6) | data formatting | bytes 5242880 | tf_op jit(solution)/shard_map/slice | solution.py:133
  256.8 4.1 %fusion.11 = f32[1,32,16,4,128]{4,1,3,2,0:T(8,128)S(1)} fusion(bf16[160,16,4,128]{3,1,0,2:T(8,128)(2,1)} %bitcast.134, f32[16,4,32,160]{3,2,1,0:T(8,128)} %copy-done.1, f32[16,4,32]{2,1,0:T(4,128)S(1)} %fusion.10, f32[16,4,32]{2,1,0:T(4,128)S(1)} %get-tuple-element.21, pred[16,32,160]{2,1,0:T(8,128)(4,1)S(1)} %broadcast_and_fusion), kind=kOutput, calls=%fused_computation.24 | convolution fusion | flops 85524480 | bytes 5079040 | tf_op jit(solution)/shard_map/nrhqk,nkrhd->nqrhd/dot_general | solution.py:93
  262.5 1.9 fusion
  264.4 2.0 copy.140
  266.4 1.1 broadcast_in_dim.40
  267.5 6.1 %all_to_all.10 = bf16[2,512,512]{1,2,0:T(8,128)(2,1)S(1)} all-to-all(bf16[2,512,512]{1,2,0:T(8,128)(2,1)S(1)} %broadcast_in_dim.40), channel_id=1, replica_groups=mesh['grp'=4,'sp'=32,'tp'=2] {'tp'}, dimensions={0} | all-to-all | bytes 2097152 | tf_op jit(solution)/shard_map/all_to_all | solution.py:23
  273.6 2.3 convolution_convert_fusion
  (81 shorter events, 8.8 us)
Async XLA Ops:
  0.0 273.6 %copy-start = (bf16[1024,1024]{1,0:T(8,128)(2,1)S(1)}, bf16[1024,1024]{1,0:T(8,128)(2,1)}, u32[]{:S(2)}) copy-start(bf16[1024,1024]{1,0:T(8,128)(2,1)} %param.9) | copy-start | bytes 6291460
  3.0 13.4 %all-to-all-start = ((bf16[2,256,2048]{2,1,0:T(8,128)(2,1)}), bf16[2,256,2048]{2,1,0:T(8,128)(2,1)}, u32[]{:S(2)}, u32[]{:S(2)}) async-start(bf16[2,256,2048]{2,1,0:T(8,128)(2,1)} %broadcast_in_dim.35), calls=%async_computation | async-start | bytes 4194304 | tf_op jit(solution)/shard_map/all_to_all | solution.py:23
  16.3 3.7 %copy-start.10 = (bf16[512,2048]{1,0:T(8,128)(2,1)S(1)}, bf16[512,2048]{1,0:T(8,128)(2,1)}, u32[]{:S(2)}) copy-start(bf16[512,2048]{1,0:T(8,128)(2,1)} %copy.142) | copy-start | bytes 6291460
  20.0 3.0 %copy-start.23 = (bf16[2048,512]{1,0:T(8,128)(2,1)S(1)}, bf16[2048,512]{1,0:T(8,128)(2,1)}, u32[]{:S(2)}) copy-start(bf16[2048,512]{1,0:T(8,128)(2,1)} %param.8) | copy-start | bytes 6291460
  28.6 41.1 %collective-permute-start = (bf16[2,512,4,128]{1,3,2,0:T(8,128)(2,1)}, bf16[2,512,4,128]{1,3,2,0:T(8,128)(2,1)}, u32[]{:S(2)}, u32[]{:S(2)}) collective-permute-start(bf16[2,512,4,128]{1,3,2,0:T(8,128)(2,1)} %pad_maximum_fusion), channel_id=1, source_target_pairs={{0,2},{2,4},{4,6},{6,8},{8,10},{10,12},{12,14},{14,16},{16,18},{18... | collective-permute-start | bytes 3145736 | tf_op jit(solution)/shard_map/ppermute | solution.py:33
  31.5 84.3 %collective-permute-start.1 = (bf16[2,512,4,128]{1,3,2,0:T(8,128)(2,1)}, bf16[2,512,4,128]{1,3,2,0:T(8,128)(2,1)}, u32[]{:S(2)}, u32[]{:S(2)}) collective-permute-start(bf16[2,512,4,128]{1,3,2,0:T(8,128)(2,1)} %pad_maximum_fusion), channel_id=1, source_target_pairs={{0,8},{2,10},{4,12},{6,14},{8,16},{10,18},{12,20},{14,22},{16,24},... | collective-permute-start | bytes 3145736 | tf_op jit(solution)/shard_map/ppermute | solution.py:33
  53.4 4.0 %copy-start.11 = (bf16[512,4,64]{2,0,1:T(8,128)(2,1)S(1)}, bf16[512,4,64]{2,0,1:T(8,128)(2,1)}, u32[]{:S(2)}) copy-start(bf16[512,4,64]{2,0,1:T(8,128)(2,1)} %copy.114) | copy-start | bytes 786436
  53.4 5.0 %copy-start.2 = (bf16[512,4,64]{2,0,1:T(8,128)(2,1)S(1)}, bf16[512,4,64]{2,0,1:T(8,128)(2,1)}, u32[]{:S(2)}) copy-start(bf16[512,4,64]{2,0,1:T(8,128)(2,1)} %copy.110) | copy-start | bytes 786436
  53.4 5.9 %copy-start.3 = (bf16[512,4,64]{2,0,1:T(8,128)(2,1)S(1)}, bf16[512,4,64]{2,0,1:T(8,128)(2,1)}, u32[]{:S(2)}) copy-start(bf16[512,4,64]{2,0,1:T(8,128)(2,1)} %copy.109) | copy-start | bytes 786436
  57.4 4.7 %copy-start.12 = (bf16[4,128,1,4,64]{1,0,4,3,2:T(4,128)(2,1)S(1)}, bf16[4,128,1,4,64]{1,0,4,3,2:T(4,128)(2,1)}, u32[]{:S(2)}) copy-start(bf16[4,128,1,4,64]{1,0,4,3,2:T(4,128)(2,1)} %concatenate.97) | copy-start | bytes 786436
  69.7 25.6 %copy-start.13 = (pred[4,128,256]{2,1,0:T(8,128)(4,1)}, pred[4,128,256]{2,1,0:T(8,128)(4,1)S(1)}, u32[]{:S(2)}) copy-start(pred[4,128,256]{2,1,0:T(8,128)(4,1)S(1)} %get-tuple-element.17) | copy-start | bytes 393220
  69.7 25.6 %copy-start.15 = (pred[4,128,256]{2,1,0:T(8,128)(4,1)}, pred[4,128,256]{2,1,0:T(8,128)(4,1)S(1)}, u32[]{:S(2)}) copy-start(pred[4,128,256]{2,1,0:T(8,128)(4,1)S(1)} %get-tuple-element.18) | copy-start | bytes 393220
  72.7 163.2 %collective-permute-start.2 = (bf16[2,1024,4,128]{1,3,2,0:T(8,128)(2,1)}, bf16[2,1024,4,128]{1,3,2,0:T(8,128)(2,1)}, u32[]{:S(2)}, u32[]{:S(2)}) collective-permute-start(bf16[2,1024,4,128]{1,3,2,0:T(8,128)(2,1)} %maximum_maximum_fusion.1), channel_id=1, source_target_pairs={{0,4},{2,6},{4,8},{6,10},{8,12},{10,14},{12,16},{14,18},{16,20},{1... | collective-permute-start | bytes 6291464 | tf_op jit(solution)/shard_map/ppermute | solution.py:33
  92.5 2.8 %copy-start.8 = (f32[4,4,128,256]{3,2,1,0:T(8,128)S(1)}, f32[4,4,128,256]{3,2,1,0:T(8,128)}, u32[]{:S(2)}) copy-start(f32[4,4,128,256]{3,2,1,0:T(8,128)} %get-tuple-element.24) | copy-start | bytes 6291460
  92.5 2.8 %copy-start.18 = (f32[4,4,128]{2,1,0:T(4,128)S(1)}, f32[4,4,128]{2,1,0:T(4,128)}, u32[]{:S(2)}) copy-start(f32[4,4,128]{2,1,0:T(4,128)} %get-tuple-element.23) | copy-start | bytes 24580
  95.3 1.7 copy-start.9
  97.0 0.6 copy-start.20
  100.6 3.2 %copy-start.16 = (pred[4,128,256]{2,1,0:T(8,128)(4,1)S(1)}, pred[4,128,256]{2,1,0:T(8,128)(4,1)}, u32[]{:S(2)}) copy-start(pred[4,128,256]{2,1,0:T(8,128)(4,1)} %copy-done.15) | copy-start | bytes 393220
  100.6 3.2 %copy-start.19 = (f32[4,4,128]{2,1,0:T(4,128)S(1)}, f32[4,4,128]{2,1,0:T(4,128)}, u32[]{:S(2)}) copy-start(f32[4,4,128]{2,1,0:T(4,128)} %get-tuple-element.23) | copy-start | bytes 24580
  100.6 3.2 %copy-start.21 = (f32[4,4,128]{2,1,0:T(4,128)S(1)}, f32[4,4,128]{2,1,0:T(4,128)}, u32[]{:S(2)}) copy-start(f32[4,4,128]{2,1,0:T(4,128)} %copy-done.20) | copy-start | bytes 24580
  106.3 5.7 %copy-start.14 = (pred[4,128,256]{2,1,0:T(8,128)(4,1)S(1)}, pred[4,128,256]{2,1,0:T(8,128)(4,1)}, u32[]{:S(2)}) copy-start(pred[4,128,256]{2,1,0:T(8,128)(4,1)} %copy-done.13) | copy-start | bytes 393220
  241.5 4.5 %copy-start.6 = (bf16[32,16,4,64]{3,0,2,1:T(8,128)(2,1)S(1)}, bf16[32,16,4,64]{3,0,2,1:T(8,128)(2,1)}, u32[]{:S(2)}) copy-start(bf16[32,16,4,64]{3,0,2,1:T(8,128)(2,1)} %copy.123) | copy-start | bytes 786436
  241.5 4.5 %copy-start.7 = (bf16[32,16,4,64]{3,0,2,1:T(8,128)(2,1)S(1)}, bf16[32,16,4,64]{3,0,2,1:T(8,128)(2,1)}, u32[]{:S(2)}) copy-start(bf16[32,16,4,64]{3,0,2,1:T(8,128)(2,1)} %copy.122) | copy-start | bytes 786436
  249.7 1.4 copy-start.1
  256.8 4.8 %copy-start.22 = (f32[512,4]{0,1:T(4,128)S(1)}, f32[512,4]{0,1:T(4,128)}, u32[]{:S(2)}) copy-start(f32[512,4]{0,1:T(4,128)} %stack_reshape.23) | copy-start | bytes 24580
  260.9 0.7 copy-start.17
  260.9 1.2 copy-start.4
  260.9 1.6 copy-start.5
where the time goes:
time: 278 us; the launch traced here: 276 us
  waiting for transfers between devices  120 us (43%)
  local copies, waits for them, and re-layouts  86.3 us (31%)
  matrix products  31.8 us (11%)
  starting transfers between devices  16.8 us (6%)
  other arithmetic  14.2 us (5%)
  blocking collectives  6.1 us (2%)
    ppermute x3, waiting for transfers between devices, passed_along(): return lax.ppermute(block, axis, route)  120 us
    slice x14, local copies, waits for them, and re-layouts, arrange(): return jnp.concatenate([whole[:-1], whole[1:]], axis=1)  26.2 us
    concatenate x14, local copies, waits for them, and re-layouts, rotate(): jnp.concatenate([first * cosine - second * sine, second * cosine + first...  19.7 us
    ppermute x3, starting transfers between devices, passed_along(): return lax.ppermute(block, axis, route)  11.4 us
    dot_general x3, matrix products, windowed(): jnp.einsum('nqrhd,nkrhd->nrhqk', query_blocks, key_blocks, preferred_elem...  10.8 us
    dot_general x3, matrix products, windowed(): jnp.einsum('nrhqk,nkrhd->nqrhd', weights, value_blocks, preferred_element...  9.11 us
    slice x2, local copies, waits for them, and re-layouts, body(): window[0]  7.15 us
    all_to_all x1, blocking collectives, sent_to_all(): return lax.all_to_all(copies, axis, split_axis=0, concat_axis=0, tiled=True)  6.1 us
  transfers between devices with their start and end apart: 4, of which 1 were waited for; matrix products, arithmetic and copies ran while one was open for 30% of the time, Pallas kernels for 0%

commit v1 on v0

v1 whole, which is shorter than its diff:
```python
import functools
import math

import jax
import jax.numpy as jnp
from jax import lax
from jax.experimental import pallas as pl
from jax.experimental.pallas import tpu as pltpu
from jax.sharding import PartitionSpec as P

HEAD = 128
REACH_STEPS = 128
MIDDLE_DILATION = 4
FAR_DILATION = 16
THETA_BASE = 500000.0

MESH = pl.DeviceIdType.MESH
F32 = jnp.float32
BF16 = jnp.bfloat16
G = MIDDLE_DILATION
T = REACH_STEPS
ROWS = G * T
NEG = -1e30
SCALE = HEAD**-0.5 * math.log2(math.e)
NT = (((1,), (1,)), ((), ()))


def iota(shape, dim):
    return lax.broadcasted_iota(jnp.int32, shape, dim)


def sin_cos(x):
    n = jnp.floor(x * (2.0 / math.pi) + 0.5)
    r = ((x - n * 1.5703125) - n * 4.837512969970703125e-4) - n * 7.549789954891882e-8
    z = r * r
    s = r + r * z * ((-1.9515295891e-4 * z + 8.3321608736e-3) * z - 1.6666654611e-1)
    c = 1.0 - 0.5 * z + z * z * ((2.443315711809948e-5 * z - 1.388731625493765e-3) * z + 4.166664568298827e-2)
    k = n.astype(jnp.int32) & 3
    odd = (k & 1) == 1
    sine = jnp.where(odd, c, s)
    cosine = jnp.where(odd, s, c)
    sine = jnp.where((k & 2) == 2, -sine, sine)
    cosine = jnp.where(((k + 1) & 2) == 2, -cosine, cosine)
    return sine, cosine


def kernel(n, tokens, wq, wk, wv, wo, out,
           x_nat, x, wq_v, wk_v, wv_v, wo_v, out_v,
           rope_c, rope_s, bias, bias2, bias3, perm_in, perm_out,
           q0, k0, v0, k1, v1, q1, q3,
           o3, l3, o3_in, l3_in, o1, l1, o1_in, l1_in,
           loc_o, loc_m, loc_l, mix_t, mixed,
           load_sem, tok_sem, k_sem, v_sem, q1_sem, q3_sem,
           o3_sem, l3_sem, o1_sem, l1_sem, mix_sem, out_sem):
    c = lax.axis_index("sp")
    tp = lax.axis_index("tp")
    heads = k0.shape[0]
    chunks = 2 * heads
    pairs = heads // 2
    half_rows = ROWS // 2

    def at(distance):
        return {"sp": lax.rem(c + distance + n, n)}

    partner = {"tp": 1 - tp}

    def load(i):
        src, dst = ((tokens, x_nat.at[tp]), (wk, wk_v), (wv, wv_v), (wq, wq_v), (wo, wo_v))[i]
        return pltpu.make_async_copy(src, dst, load_sem.at[i])

    for i in range(5):
        load(i).start()

    barrier = pltpu.get_barrier_semaphore()
    greeted = [partner, at(1), at(-1), at(2), at(-2)]
    for device in greeted:
        pl.semaphore_signal(barrier, inc=1, device_id=device, device_id_type=MESH)

    def remote(src, dst, sems, i, device):
        return pltpu.make_async_remote_copy(
            src_ref=src, dst_ref=dst, send_sem=sems.at[0, i], recv_sem=sems.at[1, i],
            device_id=device, device_id_type=MESH)

    def send_tokens():
        return remote(tokens, x_nat.at[tp], tok_sem, 0, partner)

    def send_k(h):
        return remote(k0.at[h], k1.at[h], k_sem, h, at(1))

    def send_v(h):
        return remote(v0.at[h], v1.at[h], v_sem, h, at(1))

    def chunk(ref, i):
        return ref.at[pl.ds(2 * i, 2)]

    def send_q1(i):
        return remote(chunk(q0, i), chunk(q1, i), q1_sem, i, at(-1))

    def send_q3(i):
        return remote(chunk(q1, i), chunk(q3, i), q3_sem, i, at(-2))

    def send_o3(i):
        return (remote(chunk(o3, i), chunk(o3_in, i), o3_sem, i, at(2)),
                remote(chunk(l3, i), chunk(l3_in, i), l3_sem, i, at(2)))

    def send_o1(i):
        return (remote(chunk(o1, i), chunk(o1_in, i), o1_sem, i, at(1)),
                remote(chunk(l1, i), chunk(l1_in, i), l1_sem, i, at(1)))

    def send_mixed(p):
        return remote(mixed.at[tp, p], mixed.at[tp, p], mix_sem, p, partner)

    def send_out(b):
        rows = pl.ds(b * T, T)
        return pltpu.make_async_copy(out_v.at[rows], out.at[rows], out_sem.at[b])

    pl.semaphore_wait(barrier, len(greeted))
    send_tokens().start()

    row = iota((half_rows, half_rows), 0)
    col = iota((half_rows, half_rows), 1)
    perm_in[...] = jnp.where(row == (col & (G - 1)) * (half_rows // G) + lax.shift_right_logical(col, 2), 1.0, 0.0).astype(BF16)

    lane = iota((T, HEAD), 1)
    index = lane & (HEAD // 2 - 1)
    inverse = jnp.ones((T, HEAD), F32)
    for bit in range(6):
        factor = THETA_BASE ** (-(2.0**bit) / (HEAD // 2))
        inverse = jnp.where((lax.shift_right_logical(index, bit) & 1) == 1, inverse * factor, inverse)

    @pl.loop(0, G)
    def _(g):
        position = c * ROWS + iota((T, HEAD), 0) * G + g
        sine, cosine = sin_cos(position.astype(F32) * inverse)
        rows = pl.ds(g * T, T)
        rope_c[rows, :] = cosine
        rope_s[rows, :] = jnp.where(lane < HEAD // 2, -sine, sine)

    load(0).wait()

    def permuted(u):
        half = T // 2
        y = jnp.dot(perm_in[...], x_nat[u], preferred_element_type=F32).astype(BF16)
        for g in range(G):
            x[pl.ds(g * T + u * half, half), :] = y[g * half:(g + 1) * half]

    permuted(tp)

    jk = iota((T, T), 0)
    jq = iota((T, T), 1)
    same = ((jq - jk) & (FAR_DILATION // MIDDLE_DILATION - 1)) == 0
    far = jnp.where(same, 0.0, NEG)
    bias2[...] = far + jnp.where((c + 1 < n) & (c >= 1), 0.0, NEG)
    bias3[0] = jnp.where(same & (jk >= jq), 0.0, NEG) + jnp.where((c + 3 < n) & (c >= 1), 0.0, NEG)
    bias3[1] = far + jnp.where(c + 3 < n, 0.0, NEG)

    send_tokens().wait_recv()
    permuted(1 - tp)

    def rotated(y):
        return (y * rope_c[...] + pltpu.roll(y, HEAD // 2, 1) * rope_s[...]).astype(BF16)

    load(1).wait()
    load(2).wait()
    load(3).wait()
    for p in range(pairs):
        cols = slice(2 * p * HEAD, (2 * p + 2) * HEAD)
        y = jnp.dot(x[...], wk_v[:, cols], preferred_element_type=F32)
        for s in range(2):
            k0[2 * p + s] = rotated(y[:, s * HEAD:(s + 1) * HEAD])
        y = jnp.dot(x[...], wv_v[:, cols], preferred_element_type=F32).astype(BF16)
        for s in range(2):
            v0[2 * p + s] = y[:, s * HEAD:(s + 1) * HEAD].T
            send_k(2 * p + s).start()
        y = jnp.dot(x[...], wq_v[:, cols], preferred_element_type=F32)
        for s in range(2):
            h = 2 * p + s
            send_v(h).start()
            z = rotated(y[:, s * HEAD:(s + 1) * HEAD])
            for g in range(G):
                q0[h * G + g] = z[g * T:(g + 1) * T]
        for i in range(4 * p, 4 * p + 4):
            send_q1(i).start()

    @pl.loop(0, 2 * G)
    def _(b):
        which = lax.shift_right_logical(b, 2)
        gk = b & (G - 1)

        @pl.loop(0, G)
        def _(gq):
            k_pos = (iota((T, T), 0) - T * (1 - which)) * G + gk
            d = iota((T, T), 1) * G + gq - k_pos
            ok = d >= 0
            near = jnp.where(ok & (d <= REACH_STEPS), 1, 0)
            mid = jnp.where(ok & (d <= REACH_STEPS * MIDDLE_DILATION) & ((d & (MIDDLE_DILATION - 1)) == 0), 1, 0)
            wide = jnp.where(ok & (d <= REACH_STEPS * FAR_DILATION) & ((d & (FAR_DILATION - 1)) == 0), 1, 0)
            count = near + mid + wide
            value = jnp.where(count == 3, math.log2(3.0), jnp.where(count == 2, 1.0, jnp.where(count == 1, 0.0, NEG)))
            value = value + jnp.where((which == 1) | (c >= 1), 0.0, NEG)
            bias[gq, which, pl.ds(gk * T, T), :] = value

    @pl.loop(0, G)
    def _(g):
        t = g * T + iota((T, ROWS), 0)
        s = iota((T, ROWS), 1)
        perm_out[pl.ds(g * T, T), :] = jnp.where(
            s == (t & (G - 1)) * T + lax.shift_right_logical(t, 2), 1.0, 0.0).astype(BF16)

    @pl.loop(0, chunks)
    def _(i):
        send_q1(i).wait_recv()
        send_q3(i).start()

    def softmax_of(scores):
        top = functools.reduce(jnp.maximum, [jnp.max(s, axis=0, keepdims=True) for s in scores])
        ps = [jnp.exp2(s - top) for s in scores]
        total = functools.reduce(jnp.add, [jnp.sum(p, axis=0, keepdims=True) for p in ps])
        return top, total, [p.astype(BF16) for p in ps]

    def scores_of(keys, queries, b):
        return lax.dot_general(keys, queries, NT, preferred_element_type=F32) * SCALE + b

    def tile(g):
        return pl.ds(pl.multiple_of(g * T, T), T)

    @pl.loop(0, heads)
    def _(h):
        send_k(h).wait_recv()
        send_v(h).wait_recv()

        @pl.loop(2 * h, 2 * h + 2)
        def _(i):
            send_q3(i).wait_recv()
            for s in range(2):
                t = 2 * i + s
                g = t - h * G
                q = q3[t]
                top, total, (p4, p3) = softmax_of([
                    scores_of(k1[h, tile(g), :], q, bias3[0]),
                    scores_of(k0[h, tile(g), :], q, bias3[1])])
                o = (jnp.dot(v1[h, :, tile(g)], p4, preferred_element_type=F32)
                     + jnp.dot(v0[h, :, tile(g)], p3, preferred_element_type=F32))
                o3[t] = (o * (1.0 / total)).astype(BF16)
                l3[t] = top + jnp.log2(total)
            for copy in send_o3(i):
                copy.start()

        @pl.loop(0, G)
        def _(g):
            q = q0[h * G + g]
            top, total, (p_prev, p_own) = softmax_of([
                scores_of(k1[h], q, bias[g, 0]), scores_of(k0[h], q, bias[g, 1])])
            o = (jnp.dot(v1[h], p_prev, preferred_element_type=F32)
                 + jnp.dot(v0[h], p_own, preferred_element_type=F32))
            loc_o[h * G + g] = o
            loc_m[h * G + g] = top
            loc_l[h * G + g] = total

    @pl.loop(0, chunks)
    def _(i):
        for copy in send_o3(i):
            copy.wait_recv()
        h = lax.div(i, 2)
        for s in range(2):
            t = 2 * i + s
            g = t - h * G
            top, total, (p2,) = softmax_of([scores_of(k1[h, tile(g), :], q1[t], bias2[...])])
            o = jnp.dot(v1[h, :, tile(g)], p2, preferred_element_type=F32)
            lse = l3_in[t]
            peak = jnp.maximum(top, lse)
            here = jnp.exp2(top - peak)
            there = jnp.exp2(lse - peak)
            whole = total * here + there
            o1[t] = (o * (here / whole) + o3_in[t].astype(F32) * (there / whole)).astype(BF16)
            l1[t] = peak + jnp.log2(whole)
        for copy in send_o1(i):
            copy.start()

    for p in range(pairs):
        for s in range(2):
            h = 2 * p + s
            for i in (2 * h, 2 * h + 1):
                for copy in send_o1(i):
                    copy.wait_recv()
                for t in (2 * i, 2 * i + 1):
                    top, lse = loc_m[t], l1_in[t]
                    peak = jnp.maximum(top, lse)
                    here = jnp.exp2(top - peak)
                    there = jnp.exp2(lse - peak)
                    whole = loc_l[t] * here + there
                    o = loc_o[t] * (here / whole) + o1_in[t].astype(F32) * (there / whole)
                    mix_t[h, :, (t - h * G) * T:(t - h * G + 1) * T] = o.astype(BF16)
            mixed[tp, p, :, s * HEAD:(s + 1) * HEAD] = lax.dot_general(
                perm_out[...], mix_t[h], NT, preferred_element_type=F32).astype(BF16)
        send_mixed(p).start()

    load(4).wait()
    for p in range(pairs):
        send_mixed(p).wait_recv()
    width = 2 * HEAD
    for b in range(G):
        rows = pl.ds(b * T, T)
        total = None
        for u in range(2):
            for p in range(pairs):
                start = (u * pairs + p) * width
                term = jnp.dot(mixed[u, p, rows, :], wo_v[start:start + width, :], preferred_element_type=F32)
                total = term if total is None else total + term
        out_v[rows, :] = total.astype(BF16)
        send_out(b).start()

    send_tokens().wait_send()
    for h in range(heads):
        send_k(h).wait_send()
        send_v(h).wait_send()

    @pl.loop(0, chunks)
    def _(i):
        for copy in (send_q1(i), send_q3(i), *send_o3(i), *send_o1(i)):
            copy.wait_send()

    for p in range(pairs):
        send_mixed(p).wait_send()
    for b in range(G):
        send_out(b).wait()


def body(tokens, query_weight, key_weight, value_weight, output_weight):
    n = lax.axis_size("sp")
    half_rows, depth = tokens.shape
    width = query_weight.shape[1]
    heads = width // HEAD
    tiles, chunks, pairs = heads * G, 2 * heads, heads // 2
    features = output_weight.shape[1]
    assert 2 * half_rows == ROWS and FAR_DILATION == MIDDLE_DILATION**2 and heads % 2 == 0
    assert output_weight.shape[0] == 2 * width
    vmem = pltpu.VMEM
    dma = pltpu.SemaphoreType.DMA
    square = (tiles, T, HEAD)
    stat = (tiles, 1, T)
    scratch = [
        vmem((2, half_rows, depth), BF16), vmem((ROWS, depth), BF16),
        vmem((depth, width), BF16), vmem((depth, width), BF16), vmem((depth, width), BF16),
        vmem((2 * width, features), BF16), vmem((ROWS, features), BF16),
        vmem((ROWS, HEAD), F32), vmem((ROWS, HEAD), F32),
        vmem((G, 2, ROWS, T), F32), vmem((T, T), F32), vmem((2, T, T), F32),
        vmem((half_rows, half_rows), BF16), vmem((ROWS, ROWS), BF16),
        vmem(square, BF16),
        vmem((heads, ROWS, HEAD), BF16), vmem((heads, HEAD, ROWS), BF16),
        vmem((heads, ROWS, HEAD), BF16), vmem((heads, HEAD, ROWS), BF16),
        vmem(square, BF16), vmem(square, BF16),
        vmem(square, BF16), vmem(stat, F32), vmem(square, BF16), vmem(stat, F32),
        vmem(square, BF16), vmem(stat, F32), vmem(square, BF16), vmem(stat, F32),
        vmem(square, F32), vmem(stat, F32), vmem(stat, F32),
        vmem((heads, HEAD, ROWS), BF16), vmem((2, pairs, ROWS, 2 * HEAD), BF16),
        dma((5,)), dma((2, 1)), dma((2, heads)), dma((2, heads)), dma((2, chunks)), dma((2, chunks)),
        dma((2, chunks)), dma((2, chunks)), dma((2, chunks)), dma((2, chunks)), dma((2, pairs)), dma((G,)),
    ]
    hbm = pl.BlockSpec(memory_space=pl.ANY)
    return pl.pallas_call(
        functools.partial(kernel, n),
        out_shape=jax.ShapeDtypeStruct((ROWS, features), BF16),
        in_specs=[hbm] * 5,
        out_specs=hbm,
        scratch_shapes=scratch,
        compiler_params=pltpu.CompilerParams(
            collective_id=0, has_side_effects=True, vmem_limit_bytes=60 * 1024 * 1024),
        name="attention",
    )(tokens, query_weight, key_weight, value_weight, output_weight)


def solution(mesh):
    in_specs = (
        P(("grp", "sp", "tp"), None),
        P(None, "tp"),
        P(None, "tp"),
        P(None, "tp"),
        P(None, "tp"),
    )
    out_specs = P(("grp", "sp"), "tp")
    return jax.shard_map(body, mesh=mesh, in_specs=in_specs, out_specs=out_specs, check_vma=False)
```

time: 278 us -> 98.4 us (0.35)
  the two profiles are of different devices: /device:TPU:2597 before, /device:TPU:37 now
where the time goes in v1:
time: 98.4 us; the launch traced here: 98.3 us
  Pallas kernels  96 us (98%)
  local copies, waits for them, and re-layouts  2.26 us (2%)
    pallas_call x1, Pallas kernels, body(): pl.pallas_call(functools.partial(kernel, n), out_shape=jax.ShapeDtypeStru...  96 us
    unnamed x1, local copies, waits for them, and re-layouts  2.26 us

profile of v1, /device:TPU:37, one launch (start us, length us, event | category | flops | bytes accessed | tf_op | source)
XLA Modules:
  0.0 98.3 jit_solution(8900349177716049022)
XLA Ops:
  0.0 96.0 %attention.1 = bf16[512,1024]{1,0:T(8,128)(2,1)} custom-call(bf16[256,2048]{1,0:T(8,128)(2,1)} %tokens.1, bf16[2048,512]{1,0:T(8,128)(2,1)} %wq.1, bf16[2048,512]{1,0:T(8,128)(2,1)} %wk.1, bf16[2048,512]{1,0:T(8,128)(2,1)} %wv.1, bf16[1024,1024]{1,0:T(8,128)(2,1)} %wo.1), custom_call_target="tpu_custom_call" | custom-call | tf_op jit(solution)/shard_map/attention/pallas_call | solution.py:361
  96.1 2.3 %copy.7 = bf16[512,1024]{1,0:T(8,128)(2,1)} copy(bf16[512,1024]{1,0:T(8,128)(2,1)} %attention.1) | data formatting | bytes 2097152

commit v2 on v1

v2 whole, which is shorter than its diff:
```python
import functools
import math

import jax
import jax.numpy as jnp
from jax import lax
from jax.experimental import pallas as pl
from jax.experimental.pallas import tpu as pltpu
from jax.sharding import PartitionSpec as P

HEAD = 128
REACH_STEPS = 128
MIDDLE_DILATION = 4
FAR_DILATION = 16
THETA_BASE = 500000.0

MESH = pl.DeviceIdType.MESH
F32 = jnp.float32
BF16 = jnp.bfloat16
G = MIDDLE_DILATION
T = REACH_STEPS
ROWS = G * T
NEG = -1e30
VMEM_LIMIT = 64000000
SCALE = HEAD**-0.5 * math.log2(math.e)
NT = (((1,), (1,)), ((), ()))


def iota(shape, dim):
    return lax.broadcasted_iota(jnp.int32, shape, dim)


def sin_cos(x):
    n = jnp.floor(x * (2.0 / math.pi) + 0.5)
    r = ((x - n * 1.5703125) - n * 4.837512969970703125e-4) - n * 7.549789954891882e-8
    z = r * r
    s = r + r * z * ((-1.9515295891e-4 * z + 8.3321608736e-3) * z - 1.6666654611e-1)
    c = 1.0 - 0.5 * z + z * z * ((2.443315711809948e-5 * z - 1.388731625493765e-3) * z + 4.166664568298827e-2)
    k = n.astype(jnp.int32) & 3
    odd = (k & 1) == 1
    sine = jnp.where(odd, c, s)
    cosine = jnp.where(odd, s, c)
    sine = jnp.where((k & 2) == 2, -sine, sine)
    cosine = jnp.where(((k + 1) & 2) == 2, -cosine, cosine)
    return sine, cosine


def kernel(n, tokens, wq, wk, wv, wo, out,
           x_nat, x, wq_v, wk_v, wv_v, wo_v, out_v, acc,
           rope_c, rope_s, bias, bias2, bias3, perm_in, perm_out,
           q0, k0, v0, k1, v1, v0t, v1t, q1, q3,
           o3, l3, o3_in, l3_in, o1, l1, o1_in, l1_in,
           loc_o, loc_m, loc_l, mix_t, mixed,
           load_sem, tok_sem, k_sem, v_sem, q1_sem, q3_sem,
           o3_sem, l3_sem, o1_sem, l1_sem, mix_sem, out_sem):
    c = lax.axis_index("sp")
    tp = lax.axis_index("tp")
    heads = k0.shape[0]
    width = heads * HEAD
    chunks = 2 * heads
    pairs = heads // 2
    half_rows = ROWS // 2
    piece = T // 2
    partner = {"tp": 1 - tp}

    before = [None, c >= 1, c >= 2]
    after = [None, c + 1 < n, c + 2 < n, c + 3 < n]

    def at(distance):
        return {"sp": jnp.clip(c + distance, 0, n - 1)}

    def load(i):
        src, dst = ((tokens, x_nat.at[tp]), (wk, wk_v), (wv, wv_v), (wq, wq_v), (wo, wo_v))[i]
        return pltpu.make_async_copy(src, dst, load_sem.at[i])

    for i in range(5):
        load(i).start()

    barrier = pltpu.get_barrier_semaphore()

    def greet(device):
        pl.semaphore_signal(barrier, inc=1, device_id=device, device_id_type=MESH)

    greet(partner)
    for distance in (1, 2):
        pl.when(after[distance])(functools.partial(greet, at(distance)))
        pl.when(before[distance])(functools.partial(greet, at(-distance)))

    def remote(src, dst, sems, i, device):
        return pltpu.make_async_remote_copy(
            src_ref=src, dst_ref=dst, send_sem=sems.at[0, i], recv_sem=sems.at[1, i],
            device_id=device, device_id_type=MESH)

    def send_tokens():
        return remote(tokens, x_nat.at[tp], tok_sem, 0, partner)

    def send_k(h, u):
        return remote(k0.at[h, :, u], k1.at[h, :, u], k_sem, 2 * h + u, at(1))

    def send_v(h, u):
        return remote(v0.at[h, :, u], v1.at[h, :, u], v_sem, 2 * h + u, at(1))

    def chunk(ref, i):
        return ref.at[pl.ds(2 * i, 2)]

    def send_q1(i):
        return remote(chunk(q0, i), chunk(q1, i), q1_sem, i, at(-1))

    def send_q3(i):
        return remote(chunk(q1, i), chunk(q3, i), q3_sem, i, at(-2))

    def send_o3(i):
        return (remote(chunk(o3, i), chunk(o3_in, i), o3_sem, i, at(2)),
                remote(chunk(l3, i), chunk(l3_in, i), l3_sem, i, at(2)))

    def send_o1(i):
        return (remote(chunk(o1, i), chunk(o1_in, i), o1_sem, i, at(1)),
                remote(chunk(l1, i), chunk(l1_in, i), l1_sem, i, at(1)))

    def send_mixed(h):
        return remote(mixed.at[tp, h], mixed.at[tp, h], mix_sem, h, partner)

    def send_out(b):
        rows = pl.ds(b * T, T)
        return pltpu.make_async_copy(out_v.at[rows], out.at[rows], out_sem.at[b])

    with jax.named_scope("tables"):
        row = iota((half_rows, half_rows), 0)
        col = iota((half_rows, half_rows), 1)
        perm_in[...] = jnp.where(row == (col & (G - 1)) * piece + lax.shift_right_logical(col, 2), 1.0, 0.0).astype(BF16)

        lane = iota((T, HEAD), 1)
        index = lane & (HEAD // 2 - 1)
        inverse = jnp.ones((T, HEAD), F32)
        for bit in range(6):
            factor = THETA_BASE ** (-(2.0**bit) / (HEAD // 2))
            inverse = jnp.where((lax.shift_right_logical(index, bit) & 1) == 1, inverse * factor, inverse)

        @pl.loop(0, 4)
        def _(i):
            u = lax.shift_right_logical(i, 1)
            r = iota((T, HEAD), 0) + (i & 1) * T
            local = (r & (piece - 1)) * G + lax.shift_right_logical(r, 6)
            position = c * ROWS + u * half_rows + local
            sine, cosine = sin_cos(position.astype(F32) * inverse)
            rows = pl.ds(pl.multiple_of((i & 1) * T, T), T)
            rope_c[u, rows, :] = cosine
            rope_s[u, rows, :] = jnp.where(lane < HEAD // 2, -sine, sine)

    def permuted(u):
        x[u] = jnp.dot(perm_in[...], x_nat[u], preferred_element_type=F32).astype(BF16)

    def columns(p):
        return slice(2 * p * HEAD, (2 * p + 2) * HEAD)

    def rotated(y, u):
        return (y * rope_c[u] + pltpu.roll(y, HEAD // 2, 1) * rope_s[u]).astype(BF16)

    def project(w, p, u):
        return jnp.dot(x[u], w[:, columns(p)], preferred_element_type=F32)

    def make_k(p, u):
        y = project(wk_v, p, u)
        for s in range(2):
            z = rotated(y[:, s * HEAD:(s + 1) * HEAD], u)
            for g in range(G):
                k0[2 * p + s, g, u] = z[g * piece:(g + 1) * piece]

    def make_v(p, u):
        y = project(wv_v, p, u).astype(BF16)
        for s in range(2):
            for g in range(G):
                v0[2 * p + s, g, u] = y[g * piece:(g + 1) * piece, s * HEAD:(s + 1) * HEAD]

    def forward(send, p, u):
        @pl.when(after[1])
        def _():
            for s in range(2):
                send(2 * p + s, u).start()

    with jax.named_scope("own_k"):
        load(0).wait()
        permuted(tp)
        load(1).wait()
        make_k(0, tp)

    with jax.named_scope("barrier"):
        count = 1
        for exists in (before[1], before[2], after[1], after[2]):
            count = count + exists.astype(jnp.int32)
        pl.semaphore_wait(barrier, count)
        send_tokens().start()

    with jax.named_scope("own_kv"):
        forward(send_k, 0, tp)
        load(2).wait()
        make_v(0, tp)
        forward(send_v, 0, tp)
        make_k(1, tp)
        forward(send_k, 1, tp)
        make_v(1, tp)
        forward(send_v, 1, tp)

    @pl.when(c < 1)
    def _():
        k1[...] = jnp.zeros_like(k1)
        v1[...] = jnp.zeros_like(v1)

    @pl.when(c < 2)
    def _():
        o3_in[...] = jnp.zeros_like(o3_in)
        l3_in[...] = jnp.full_like(l3_in, NEG)
        o1_in[...] = jnp.zeros_like(o1_in)
        l1_in[...] = jnp.full_like(l1_in, NEG)

    with jax.named_scope("tokwait"):
        send_tokens().wait_recv()

    with jax.named_scope("other_kv"):
        permuted(1 - tp)
        for p in range(pairs):
            make_k(p, 1 - tp)
            forward(send_k, p, 1 - tp)
            make_v(p, 1 - tp)
            forward(send_v, p, 1 - tp)

    with jax.named_scope("q"):
        load(3).wait()
        for p in range(pairs):
            y = jnp.dot(x[...].reshape(ROWS, x.shape[2]), wq_v[:, columns(p)], preferred_element_type=F32)
            for s in range(2):
                for u in range(2):
                    z = rotated(y[u * half_rows:(u + 1) * half_rows, s * HEAD:(s + 1) * HEAD], u)
                    for g in range(G):
                        q0[(2 * p + s) * G + g, u] = z[g * piece:(g + 1) * piece]
            if p == 0:
                @pl.when(before[2])
                def _():
                    for i in range(chunks // 2):
                        send_q1(i).start()

    with jax.named_scope("bias"):
        jk = iota((T, T), 0)
        jq = iota((T, T), 1)
        same = ((jq - jk) & (FAR_DILATION // MIDDLE_DILATION - 1)) == 0
        far = jnp.where(same, 0.0, NEG)
        bias2[...] = far
        bias3[0] = jnp.where(same & (jk >= jq), 0.0, NEG) + jnp.where(before[1], 0.0, NEG)
        bias3[1] = far

        @pl.loop(0, 2 * G)
        def _(b):
            which = lax.shift_right_logical(b, 2)
            gk = b & (G - 1)

            @pl.loop(0, G)
            def _(gq):
                k_pos = (iota((T, T), 0) - T * (1 - which)) * G + gk
                d = iota((T, T), 1) * G + gq - k_pos
                ok = d >= 0
                near = jnp.where(ok & (d <= REACH_STEPS), 1, 0)
                mid = jnp.where(ok & (d <= REACH_STEPS * MIDDLE_DILATION) & ((d & (MIDDLE_DILATION - 1)) == 0), 1, 0)
                wide = jnp.where(ok & (d <= REACH_STEPS * FAR_DILATION) & ((d & (FAR_DILATION - 1)) == 0), 1, 0)
                times = near + mid + wide
                value = jnp.where(times == 3, math.log2(3.0), jnp.where(times == 2, 1.0, jnp.where(times == 1, 0.0, NEG)))
                value = value + jnp.where((which == 1) | before[1], 0.0, NEG)
                bias[gq, which, pl.ds(pl.multiple_of(gk * T, T), T), :] = value

    with jax.named_scope("fwdq"):
        def pass_on(i):
            @pl.when(before[1] & after[1])
            def _():
                send_q1(i).wait_recv()

                @pl.when(before[2])
                def _():
                    send_q3(i).start()

        @pl.loop(0, chunks // 2)
        def _(i):
            pass_on(i)

            @pl.when(before[2])
            def _():
                send_q1(chunks // 2 + i).start()

        @pl.loop(0, G)
        def _(g):
            t = g * T + iota((T, ROWS), 0)
            s = iota((T, ROWS), 1)
            perm_out[pl.ds(pl.multiple_of(g * T, T), T), :] = jnp.where(
                s == (t & (G - 1)) * T + lax.shift_right_logical(t, 2), 1.0, 0.0).astype(BF16)

        for h in range(heads):
            v0t[h] = v0[h].reshape(ROWS, HEAD).T

        @pl.loop(chunks // 2, chunks)
        def _(i):
            pass_on(i)

    def softmax_of(scores):
        top = functools.reduce(jnp.maximum, [jnp.max(s, axis=0, keepdims=True) for s in scores])
        ps = [jnp.exp2(s - top) for s in scores]
        total = functools.reduce(jnp.add, [jnp.sum(p, axis=0, keepdims=True) for p in ps])
        return top, total, [p.astype(BF16) for p in ps]

    def scores_of(keys, queries, b):
        return lax.dot_general(keys, queries, NT, preferred_element_type=F32) * SCALE + b

    def tile(g):
        return pl.ds(pl.multiple_of(g * T, T), T)

    def rows_of(ref, *where):
        return ref[where].reshape(-1, HEAD)

    with jax.named_scope("o3local"):
        @pl.loop(0, heads)
        def _(h):
            @pl.when(before[1])
            def _():
                for u in range(2):
                    send_k(h, u).wait_recv()
                    send_v(h, u).wait_recv()

            v1t[h] = rows_of(v1, h).T

            @pl.when(after[3])
            def _():
                @pl.loop(2 * h, 2 * h + 2)
                def _(i):
                    send_q3(i).wait_recv()
                    for s in range(2):
                        t = 2 * i + s
                        g = t - h * G
                        q = rows_of(q3, t)
                        top, total, (p4, p3) = softmax_of([
                            scores_of(rows_of(k1, h, g), q, bias3[0]),
                            scores_of(rows_of(k0, h, g), q, bias3[1])])
                        o = (jnp.dot(v1t[h, :, tile(g)], p4, preferred_element_type=F32)
                             + jnp.dot(v0t[h, :, tile(g)], p3, preferred_element_type=F32))
                        o3[t] = (o * (1.0 / total)).astype(BF16)
                        l3[t] = top + jnp.log2(total)
                    for copy in send_o3(i):
                        copy.start()

            @pl.loop(0, G)
            def _(g):
                q = rows_of(q0, h * G + g)
                top, total, (p_prev, p_own) = softmax_of([
                    scores_of(rows_of(k1, h), q, bias[g, 0]), scores_of(rows_of(k0, h), q, bias[g, 1])])
                o = (jnp.dot(v1t[h], p_prev, preferred_element_type=F32)
                     + jnp.dot(v0t[h], p_own, preferred_element_type=F32))
                loc_o[h * G + g] = o
                loc_m[h * G + g] = top
                loc_l[h * G + g] = total

    with jax.named_scope("o1"):
        @pl.when(before[1] & after[1])
        def _():
            @pl.loop(0, chunks)
            def _(i):
                @pl.when(before[2])
                def _():
                    for copy in send_o3(i):
                        copy.wait_recv()

                h = lax.div(i, 2)
                for s in range(2):
                    t = 2 * i + s
                    g = t - h * G
                    top, total, (p2,) = softmax_of([scores_of(rows_of(k1, h, g), rows_of(q1, t), bias2[...])])
                    o = jnp.dot(v1t[h, :, tile(g)], p2, preferred_element_type=F32)
                    lse = l3_in[t]
                    peak = jnp.maximum(top, lse)
                    here = jnp.exp2(top - peak)
                    there = jnp.exp2(lse - peak)
                    whole = total * here + there
                    o1[t] = (o * (here / whole) + o3_in[t].astype(F32) * (there / whole)).astype(BF16)
                    l1[t] = peak + jnp.log2(whole)
                for copy in send_o1(i):
                    copy.start()

    def row_block(b):
        return slice(b * T, (b + 1) * T)

    def term(u, h, b):
        start = pl.multiple_of(u * width + h * HEAD, HEAD)
        return jnp.dot(mixed[u, h, row_block(b), :], wo_v[pl.ds(start, HEAD), :], preferred_element_type=F32)

    with jax.named_scope("final"):
        load(4).wait()
        for h in range(heads):
            with jax.named_scope(f"head{h}"):
                @pl.when(before[2])
                def _():
                    for i in (2 * h, 2 * h + 1):
                        for copy in send_o1(i):
                            copy.wait_recv()

                for g in range(G):
                    t = h * G + g
                    top, lse = loc_m[t], l1_in[t]
                    peak = jnp.maximum(top, lse)
                    here = jnp.exp2(top - peak)
                    there = jnp.exp2(lse - peak)
                    whole = loc_l[t] * here + there
                    o = loc_o[t] * (here / whole) + o1_in[t].astype(F32) * (there / whole)
                    mix_t[h, :, g * T:(g + 1) * T] = o.astype(BF16)
                mixed[tp, h] = lax.dot_general(perm_out[...], mix_t[h], NT, preferred_element_type=F32).astype(BF16)
                send_mixed(h).start()
            with jax.named_scope(f"acc{h}"):
                for b in range(G):
                    y = term(tp, h, b)
                    acc[row_block(b)] = y if h == 0 else acc[row_block(b)] + y
                if h > 0:
                    send_mixed(h - 1).wait_recv()
                    for b in range(G):
                        acc[row_block(b)] += term(1 - tp, h - 1, b)

    with jax.named_scope("out"):
        send_mixed(heads - 1).wait_recv()
        for b in range(G):
            out_v[row_block(b)] = (acc[row_block(b)] + term(1 - tp, heads - 1, b)).astype(BF16)
            send_out(b).start()

    with jax.named_scope("drain"):
        send_tokens().wait_send()

        @pl.when(after[1])
        def _():
            for h in range(heads):
                for u in range(2):
                    send_k(h, u).wait_send()
                    send_v(h, u).wait_send()

        @pl.loop(0, chunks)
        def _(i):
            @pl.when(before[2])
            def _():
                send_q1(i).wait_send()

            @pl.when(before[2] & after[1])
            def _():
                send_q3(i).wait_send()

            @pl.when(after[3])
            def _():
                for copy in send_o3(i):
                    copy.wait_send()

            @pl.when(before[1] & after[1])
            def _():
                for copy in send_o1(i):
                    copy.wait_send()

        for h in range(heads):
            send_mixed(h).wait_send()
        for b in range(G):
            send_out(b).wait()


def body(tokens, query_weight, key_weight, value_weight, output_weight):
    n = lax.axis_size("sp")
    half_rows, depth = tokens.shape
    width = query_weight.shape[1]
    heads = width // HEAD
    tiles, chunks = heads * G, 2 * heads
    features = output_weight.shape[1]
    assert 2 * half_rows == ROWS and FAR_DILATION == MIDDLE_DILATION**2 and heads % 2 == 0
    assert output_weight.shape[0] == 2 * width
    vmem = pltpu.VMEM
    dma = pltpu.SemaphoreType.DMA
    split = (tiles, 2, T // 2, HEAD)
    by_head = (heads, G, 2, T // 2, HEAD)
    turned = (heads, HEAD, ROWS)
    square = (tiles, T, HEAD)
    stat = (tiles, 1, T)
    scratch = [
        vmem((2, half_rows, depth), BF16), vmem((2, half_rows, depth), BF16),
        vmem((depth, width), BF16), vmem((depth, width), BF16), vmem((depth, width), BF16),
        vmem((2 * width, features), BF16), vmem((ROWS, features), BF16), vmem((ROWS, features), F32),
        vmem((2, half_rows, HEAD), F32), vmem((2, half_rows, HEAD), F32),
        vmem((G, 2, ROWS, T), F32), vmem((T, T), F32), vmem((2, T, T), F32),
        vmem((half_rows, half_rows), BF16), vmem((ROWS, ROWS), BF16),
        vmem(split, BF16),
        vmem(by_head, BF16), vmem(by_head, BF16), vmem(by_head, BF16), vmem(by_head, BF16),
        vmem(turned, BF16), vmem(turned, BF16),
        vmem(split, BF16), vmem(split, BF16),
        vmem(square, BF16), vmem(stat, F32), vmem(square, BF16), vmem(stat, F32),
        vmem(square, BF16), vmem(stat, F32), vmem(square, BF16), vmem(stat, F32),
        vmem(square, F32), vmem(stat, F32), vmem(stat, F32),
        vmem(turned, BF16), vmem((2, heads, ROWS, HEAD), BF16),
        dma((5,)), dma((2, 1)), dma((2, chunks)), dma((2, chunks)), dma((2, chunks)), dma((2, chunks)),
        dma((2, chunks)), dma((2, chunks)), dma((2, chunks)), dma((2, chunks)), dma((2, heads)), dma((G,)),
    ]
    hbm = pl.BlockSpec(memory_space=pltpu.HBM)
    return pl.pallas_call(
        functools.partial(kernel, n),
        out_shape=jax.ShapeDtypeStruct((ROWS, features), BF16),
        in_specs=[hbm] * 5,
        out_specs=pl.BlockSpec(memory_space=pl.ANY),
        scratch_shapes=scratch,
        compiler_params=pltpu.CompilerParams(
            collective_id=0, has_side_effects=True, vmem_limit_bytes=VMEM_LIMIT),
        name="attention",
    )(tokens, query_weight, key_weight, value_weight, output_weight)


def solution(mesh):
    in_specs = (
        P(("grp", "sp", "tp"), None),
        P(None, "tp"),
        P(None, "tp"),
        P(None, "tp"),
        P(None, "tp"),
    )
    out_specs = P(("grp", "sp"), "tp")
    return jax.shard_map(body, mesh=mesh, in_specs=in_specs, out_specs=out_specs, check_vma=False)
```

time: 98.4 us -> 91.9 us (0.934)
  the two profiles are of different devices: /device:TPU:37 before, /device:TPU:293 now
where the time goes in v2:
time: 91.9 us; the launch traced here: 91.8 us
  Pallas kernels  89.5 us (97%)
  local copies, waits for them, and re-layouts  2.26 us (2%)
    pallas_call x1, Pallas kernels, body(): pl.pallas_call(functools.partial(kernel, n), out_shape=jax.ShapeDtypeStru...  89.5 us
    unnamed x1, local copies, waits for them, and re-layouts  2.26 us

profile of v2, /device:TPU:293, one launch (start us, length us, event | category | flops | bytes accessed | tf_op | source)
XLA Modules:
  0.0 91.8 jit_solution(6043295610727029087)
XLA Ops:
  0.0 89.5 %attention.1 = bf16[512,1024]{1,0:T(8,128)(2,1)} custom-call(bf16[256,2048]{1,0:T(8,128)(2,1)} %tokens.1, bf16[2048,512]{1,0:T(8,128)(2,1)} %wq.1, bf16[2048,512]{1,0:T(8,128)(2,1)} %wk.1, bf16[2048,512]{1,0:T(8,128)(2,1)} %wv.1, bf16[1024,1024]{1,0:T(8,128)(2,1)} %wo.1), custom_call_target="tpu_custom_call" | custom-call | tf_op jit(solution)/shard_map/attention/pallas_call | solution.py:497
  89.5 2.3 %copy.7 = bf16[512,1024]{1,0:T(8,128)(2,1)} copy(bf16[512,1024]{1,0:T(8,128)(2,1)} %attention.1) | data formatting | bytes 2097152

commit v3 on v2

--- a/solution.py
+++ b/solution.py
@@ -21,7 +21,7 @@
 T = REACH_STEPS
 ROWS = G * T
 NEG = -1e30
-VMEM_LIMIT = 64000000
+VMEM_LIMIT = 55_000_000
 SCALE = HEAD**-0.5 * math.log2(math.e)
 NT = (((1,), (1,)), ((), ()))
 
@@ -196,10 +196,6 @@
         load(2).wait()
         make_v(0, tp)
         forward(send_v, 0, tp)
-        make_k(1, tp)
-        forward(send_k, 1, tp)
-        make_v(1, tp)
-        forward(send_v, 1, tp)
 
     @pl.when(c < 1)
     def _():
@@ -213,31 +209,51 @@
         o1_in[...] = jnp.zeros_like(o1_in)
         l1_in[...] = jnp.full_like(l1_in, NEG)
 
+    def make_q(p):
+        y = jnp.dot(x[...].reshape(ROWS, x.shape[2]), wq_v[:, columns(p)], preferred_element_type=F32)
+        for s in range(2):
+            for u in range(2):
+                z = rotated(y[u * half_rows:(u + 1) * half_rows, s * HEAD:(s + 1) * HEAD], u)
+                for g in range(G):
+                    q0[(2 * p + s) * G + g, u] = z[g * piece:(g + 1) * piece]
+
+    half = chunks // 2
+
+    def ask(p):
+        @pl.when(before[2])
+        def _():
+            for i in range(p * half, (p + 1) * half):
+                send_q1(i).start()
+
+    with jax.named_scope("own_kv1"):
+        make_k(1, tp)
+
     with jax.named_scope("tokwait"):
         send_tokens().wait_recv()
 
-    with jax.named_scope("other_kv"):
+    with jax.named_scope("other_kv0"):
         permuted(1 - tp)
-        for p in range(pairs):
-            make_k(p, 1 - tp)
-            forward(send_k, p, 1 - tp)
-            make_v(p, 1 - tp)
-            forward(send_v, p, 1 - tp)
-
-    with jax.named_scope("q"):
+        make_k(0, 1 - tp)
+        forward(send_k, 0, 1 - tp)
+        make_v(0, 1 - tp)
+        forward(send_v, 0, 1 - tp)
+        forward(send_k, 1, tp)
+
+    with jax.named_scope("q0"):
         load(3).wait()
-        for p in range(pairs):
-            y = jnp.dot(x[...].reshape(ROWS, x.shape[2]), wq_v[:, columns(p)], preferred_element_type=F32)
-            for s in range(2):
-                for u in range(2):
-                    z = rotated(y[u * half_rows:(u + 1) * half_rows, s * HEAD:(s + 1) * HEAD], u)
-                    for g in range(G):
-                        q0[(2 * p + s) * G + g, u] = z[g * piece:(g + 1) * piece]
-            if p == 0:
-                @pl.when(before[2])
-                def _():
-                    for i in range(chunks // 2):
-                        send_q1(i).start()
+        make_q(0)
+        ask(0)
+
+    with jax.named_scope("kv1"):
+        make_v(1, tp)
+        forward(send_v, 1, tp)
+        make_k(1, 1 - tp)
+        forward(send_k, 1, 1 - tp)
+        make_v(1, 1 - tp)
+        forward(send_v, 1, 1 - tp)
+
+    with jax.named_scope("q1"):
+        make_q(1)
 
     with jax.named_scope("bias"):
         jk = iota((T, T), 0)
@@ -266,23 +282,21 @@
                 value = value + jnp.where((which == 1) | before[1], 0.0, NEG)
                 bias[gq, which, pl.ds(pl.multiple_of(gk * T, T), T), :] = value
 
+    def pass_on(i):
+        @pl.when(before[1] & after[1])
+        def _():
+            send_q1(i).wait_recv()
+
+            @pl.when(before[2])
+            def _():
+                send_q3(i).start()
+
     with jax.named_scope("fwdq"):
-        def pass_on(i):
-            @pl.when(before[1] & after[1])
-            def _():
-                send_q1(i).wait_recv()
-
-                @pl.when(before[2])
-                def _():
-                    send_q3(i).start()
-
-        @pl.loop(0, chunks // 2)
+        @pl.loop(0, half)
         def _(i):
             pass_on(i)
 
-            @pl.when(before[2])
-            def _():
-                send_q1(chunks // 2 + i).start()
+        ask(1)
 
         @pl.loop(0, G)
         def _(g):
@@ -294,10 +308,6 @@
         for h in range(heads):
             v0t[h] = v0[h].reshape(ROWS, HEAD).T
 
-        @pl.loop(chunks // 2, chunks)
-        def _(i):
-            pass_on(i)
-
     def softmax_of(scores):
         top = functools.reduce(jnp.maximum, [jnp.max(s, axis=0, keepdims=True) for s in scores])
         ps = [jnp.exp2(s - top) for s in scores]
@@ -313,72 +323,96 @@
     def rows_of(ref, *where):
         return ref[where].reshape(-1, HEAD)
 
-    with jax.named_scope("o3local"):
-        @pl.loop(0, heads)
+    def context(h):
+        @pl.when(before[1])
+        def _():
+            for u in range(2):
+                send_k(h, u).wait_recv()
+                send_v(h, u).wait_recv()
+
+        v1t[h] = rows_of(v1, h).T
+
+    def widest(i):
+        h = lax.div(i, 2)
+
+        @pl.when(after[3])
+        def _():
+            send_q3(i).wait_recv()
+            for s in range(2):
+                t = 2 * i + s
+                g = t - h * G
+                q = rows_of(q3, t)
+                top, total, (p4, p3) = softmax_of([
+                    scores_of(rows_of(k1, h, g), q, bias3[0]),
+                    scores_of(rows_of(k0, h, g), q, bias3[1])])
+                o = (jnp.dot(v1t[h, :, tile(g)], p4, preferred_element_type=F32)
+                     + jnp.dot(v0t[h, :, tile(g)], p3, preferred_element_type=F32))
+                o3[t] = (o * (1.0 / total)).astype(BF16)
+                l3[t] = top + jnp.log2(total)
+            for copy in send_o3(i):
+                copy.start()
+
+    def local(h):
+        @pl.loop(0, G)
+        def _(g):
+            q = rows_of(q0, h * G + g)
+            top, total, (p_prev, p_own) = softmax_of([
+                scores_of(rows_of(k1, h), q, bias[g, 0]), scores_of(rows_of(k0, h), q, bias[g, 1])])
+            o = (jnp.dot(v1t[h], p_prev, preferred_element_type=F32)
+                 + jnp.dot(v0t[h], p_own, preferred_element_type=F32))
+            loc_o[h * G + g] = o
+            loc_m[h * G + g] = top
+            loc_l[h * G + g] = total
+
+    def answer(i):
+        @pl.when(before[1] & after[1])
+        def _():
+            @pl.when(before[2])
+            def _():
+                for copy in send_o3(i):
+                    copy.wait_recv()
+
+            h = lax.div(i, 2)
+            for s in range(2):
+                t = 2 * i + s
+                g = t - h * G
+                top, total, (p2,) = softmax_of([scores_of(rows_of(k1, h, g), rows_of(q1, t), bias2[...])])
+                o = jnp.dot(v1t[h, :, tile(g)], p2, preferred_element_type=F32)
+                lse = l3_in[t]
+                peak = jnp.maximum(top, lse)
+                here = jnp.exp2(top - peak)
+                there = jnp.exp2(lse - peak)
+                whole = total * here + there
+                o1[t] = (o * (here / whole) + o3_in[t].astype(F32) * (there / whole)).astype(BF16)
+                l1[t] = peak + jnp.log2(whole)
+            for copy in send_o1(i):
+                copy.start()
+
+    with jax.named_scope("ctx01_o3"):
+        @pl.loop(0, heads // 2)
         def _(h):
-            @pl.when(before[1])
-            def _():
-                for u in range(2):
-                    send_k(h, u).wait_recv()
-                    send_v(h, u).wait_recv()
-
-            v1t[h] = rows_of(v1, h).T
-
-            @pl.when(after[3])
-            def _():
-                @pl.loop(2 * h, 2 * h + 2)
-                def _(i):
-                    send_q3(i).wait_recv()
-                    for s in range(2):
-                        t = 2 * i + s
-                        g = t - h * G
-                        q = rows_of(q3, t)
-                        top, total, (p4, p3) = softmax_of([
-                            scores_of(rows_of(k1, h, g), q, bias3[0]),
-                            scores_of(rows_of(k0, h, g), q, bias3[1])])
-                        o = (jnp.dot(v1t[h, :, tile(g)], p4, preferred_element_type=F32)
-                             + jnp.dot(v0t[h, :, tile(g)], p3, preferred_element_type=F32))
-                        o3[t] = (o * (1.0 / total)).astype(BF16)
-                        l3[t] = top + jnp.log2(total)
-                    for copy in send_o3(i):
-                        copy.start()
-
-            @pl.loop(0, G)
-            def _(g):
-                q = rows_of(q0, h * G + g)
-                top, total, (p_prev, p_own) = softmax_of([
-                    scores_of(rows_of(k1, h), q, bias[g, 0]), scores_of(rows_of(k0, h), q, bias[g, 1])])
-                o = (jnp.dot(v1t[h], p_prev, preferred_element_type=F32)
-                     + jnp.dot(v0t[h], p_own, preferred_element_type=F32))
-                loc_o[h * G + g] = o
-                loc_m[h * G + g] = top
-                loc_l[h * G + g] = total
-
-    with jax.named_scope("o1"):
-        @pl.when(before[1] & after[1])
-        def _():
-            @pl.loop(0, chunks)
-            def _(i):
-                @pl.when(before[2])
-                def _():
-                    for copy in send_o3(i):
-                        copy.wait_recv()
-
-                h = lax.div(i, 2)
-                for s in range(2):
-                    t = 2 * i + s
-                    g = t - h * G
-                    top, total, (p2,) = softmax_of([scores_of(rows_of(k1, h, g), rows_of(q1, t), bias2[...])])
-                    o = jnp.dot(v1t[h, :, tile(g)], p2, preferred_element_type=F32)
-                    lse = l3_in[t]
-                    peak = jnp.maximum(top, lse)
-                    here = jnp.exp2(top - peak)
-                    there = jnp.exp2(lse - peak)
-                    whole = total * here + there
-                    o1[t] = (o * (here / whole) + o3_in[t].astype(F32) * (there / whole)).astype(BF16)
-                    l1[t] = peak + jnp.log2(whole)
-                for copy in send_o1(i):
-                    copy.start()
+            context(h)
+            for s in range(2):
+                widest(2 * h + s)
+
+    with jax.named_scope("local01_fwd"):
+        @pl.loop(0, heads // 2)
+        def _(h):
+            local(h)
+            for s in range(2):
+                pass_on(half + 2 * h + s)
+
+    with jax.named_scope("ctx23_local"):
+        @pl.loop(heads // 2, heads)
+        def _(h):
+            context(h)
+            local(h)
+
+    with jax.named_scope("o1_o3"):
+        @pl.loop(0, half)
+        def _(i):
+            answer(i)
+            widest(half + i)
 
     def row_block(b):
         return slice(b * T, (b + 1) * T)
@@ -387,35 +421,48 @@
         start = pl.multiple_of(u * width + h * HEAD, HEAD)
         return jnp.dot(mixed[u, h, row_block(b), :], wo_v[pl.ds(start, HEAD), :], preferred_element_type=F32)
 
+    def finish(h):
+        with jax.named_scope(f"head{h}"):
+            @pl.when(before[2])
+            def _():
+                for i in (2 * h, 2 * h + 1):
+                    for copy in send_o1(i):
+                        copy.wait_recv()
+
+            for g in range(G):
+                t = h * G + g
+                top, lse = loc_m[t], l1_in[t]
+                peak = jnp.maximum(top, lse)
+                here = jnp.exp2(top - peak)
+                there = jnp.exp2(lse - peak)
+                whole = loc_l[t] * here + there
+                o = loc_o[t] * (here / whole) + o1_in[t].astype(F32) * (there / whole)
+                mix_t[h, :, g * T:(g + 1) * T] = o.astype(BF16)
+            mixed[tp, h] = lax.dot_general(perm_out[...], mix_t[h], NT, preferred_element_type=F32).astype(BF16)
+            send_mixed(h).start()
+        with jax.named_scope(f"acc{h}"):
+            for b in range(G):
+                y = term(tp, h, b)
+                acc[row_block(b)] = y if h == 0 else acc[row_block(b)] + y
+            if h > 0:
+                send_mixed(h - 1).wait_recv()
+                for b in range(G):
+                    acc[row_block(b)] += term(1 - tp, h - 1, b)
+
+    load(4).wait()
     with jax.named_scope("final"):
-        load(4).wait()
-        for h in range(heads):
-            with jax.named_scope(f"head{h}"):
-                @pl.when(before[2])
-                def _():
-                    for i in (2 * h, 2 * h + 1):
-                        for copy in send_o1(i):
-                            copy.wait_recv()
-
-                for g in range(G):
-                    t = h * G + g
-                    top, lse = loc_m[t], l1_in[t]
-                    peak = jnp.maximum(top, lse)
-                    here = jnp.exp2(top - peak)
-                    there = jnp.exp2(lse - peak)
-                    whole = loc_l[t] * here + there
-                    o = loc_o[t] * (here / whole) + o1_in[t].astype(F32) * (there / whole)
-                    mix_t[h, :, g * T:(g + 1) * T] = o.astype(BF16)
-                mixed[tp, h] = lax.dot_general(perm_out[...], mix_t[h], NT, preferred_element_type=F32).astype(BF16)
-                send_mixed(h).start()
-            with jax.named_scope(f"acc{h}"):
-                for b in range(G):
-                    y = term(tp, h, b)
-                    acc[row_block(b)] = y if h == 0 else acc[row_block(b)] + y
-                if h > 0:
-                    send_mixed(h - 1).wait_recv()
-                    for b in range(G):
-                        acc[row_block(b)] += term(1 - tp, h - 1, b)
+        finish(0)
+    with jax.named_scope("o1b"):
+        for i in (half, half + 1):
+            answer(jnp.int32(i))
+    with jax.named_scope("finalb"):
+        finish(1)
+    with jax.named_scope("o1c"):
+        for i in range(half + 2, chunks):
+            answer(jnp.int32(i))
+    with jax.named_scope("finalc"):
+        for h in range(2, heads):
+            finish(h)
 
     with jax.named_scope("out"):
         send_mixed(heads - 1).wait_recv()

time: 91.9 us -> 84.9 us (0.924)
  Pallas kernels: 89.5 us -> 83.9 us
  local copies, waits for them, and re-layouts: 2.26 us -> 0.97 us
    pallas_call x1, Pallas kernels: 89.5 us -> 83.9 us  [body(): pl.pallas_call(functools.partial(kernel, n), out_shape=jax.ShapeDtypeStru...]
    unnamed x1, local copies, waits for them, and re-layouts: 2.26 us -> 0.97 us
where the time goes in v3:
time: 84.9 us
  Pallas kernels  83.9 us (99%)
  local copies, waits for them, and re-layouts  0.97 us (1%)
    pallas_call x1, Pallas kernels, body(): pl.pallas_call(functools.partial(kernel, n), out_shape=jax.ShapeDtypeStru...  83.9 us

profile of v3, /device:TPU:293, one launch (start us, length us, event | category | flops | bytes accessed | tf_op | source)
XLA Modules:
  0.0 84.9 jit_solution(8297510248521359483)
XLA Ops:
  0.0 83.9 %attention.1 = bf16[512,1024]{1,0:T(8,128)(2,1)S(1)} custom-call(bf16[256,2048]{1,0:T(8,128)(2,1)} %tokens.1, bf16[2048,512]{1,0:T(8,128)(2,1)} %wq.1, bf16[2048,512]{1,0:T(8,128)(2,1)} %wk.1, bf16[2048,512]{1,0:T(8,128)(2,1)} %wv.1, bf16[1024,1024]{1,0:T(8,128)(2,1)} %wo.1), custom_call_target="tpu_custom_call" | custom-call | tf_op jit(solution)/shard_map/attention/pallas_call | solution.py:544
  83.9 1.0 %copy.7 = bf16[512,1024]{1,0:T(8,128)(2,1)} copy(bf16[512,1024]{1,0:T(8,128)(2,1)S(1)} %attention.1) | data formatting | bytes 2097152

commit v4 on v3

--- a/solution.py
+++ b/solution.py
@@ -48,11 +48,11 @@
 def kernel(n, tokens, wq, wk, wv, wo, out,
            x_nat, x, wq_v, wk_v, wv_v, wo_v, out_v, acc,
            rope_c, rope_s, bias, bias2, bias3, perm_in, perm_out,
-           q0, k0, v0, k1, v1, v0t, v1t, q1, q3,
+           q0, k0, v0, k1, v1, v0t, v1t, q1, q3, qx, ox, lx,
            o3, l3, o3_in, l3_in, o1, l1, o1_in, l1_in,
            loc_o, loc_m, loc_l, mix_t, mixed,
            load_sem, tok_sem, k_sem, v_sem, q1_sem, q3_sem,
-           o3_sem, l3_sem, o1_sem, l1_sem, mix_sem, out_sem):
+           o3_sem, l3_sem, o1_sem, l1_sem, qx_sem, ox_sem, mix_sem, out_sem):
     c = lax.axis_index("sp")
     tp = lax.axis_index("tp")
     heads = k0.shape[0]
@@ -63,7 +63,7 @@
     piece = T // 2
     partner = {"tp": 1 - tp}
 
-    before = [None, c >= 1, c >= 2]
+    before = [None, c >= 1, c >= 2, c >= 3]
     after = [None, c + 1 < n, c + 2 < n, c + 3 < n]
 
     def at(distance):
@@ -82,9 +82,10 @@
         pl.semaphore_signal(barrier, inc=1, device_id=device, device_id_type=MESH)
 
     greet(partner)
-    for distance in (1, 2):
-        pl.when(after[distance])(functools.partial(greet, at(distance)))
-        pl.when(before[distance])(functools.partial(greet, at(-distance)))
+    pl.when(before[1])(functools.partial(greet, at(-1)))
+    pl.when(before[3])(functools.partial(greet, at(-2)))
+    pl.when(before[1] & after[1])(functools.partial(greet, at(1)))
+    pl.when(before[1] & after[2])(functools.partial(greet, at(2)))
 
     def remote(src, dst, sems, i, device):
         return pltpu.make_async_remote_copy(
@@ -108,6 +109,16 @@
 
     def send_q3(i):
         return remote(chunk(q1, i), chunk(q3, i), q3_sem, i, at(-2))
+
+    def send_qx(i):
+        return remote(chunk(q1, i), chunk(qx, i), qx_sem, i, at(-1))
+
+    def send_ox(i):
+        return tuple(
+            pltpu.make_async_remote_copy(
+                src_ref=chunk(src, i), dst_ref=chunk(dst, i), send_sem=ox_sem.at[k, i], recv_sem=sems.at[1, i],
+                device_id=at(1), device_id_type=MESH)
+            for k, (src, dst, sems) in enumerate(((ox, o3_in, o3_sem), (lx, l3_in, l3_sem))))
 
     def send_o3(i):
         return (remote(chunk(o3, i), chunk(o3_in, i), o3_sem, i, at(2)),
@@ -186,7 +197,7 @@
 
     with jax.named_scope("barrier"):
         count = 1
-        for exists in (before[1], before[2], after[1], after[2]):
+        for exists in (after[1], before[2], before[1] & after[2], before[3]):
             count = count + exists.astype(jnp.int32)
         pl.semaphore_wait(barrier, count)
         send_tokens().start()
@@ -287,9 +298,13 @@
         def _():
             send_q1(i).wait_recv()
 
-            @pl.when(before[2])
+            @pl.when(before[3])
             def _():
                 send_q3(i).start()
+
+            @pl.when(c == 2)
+            def _():
+                send_qx(i).start()
 
     with jax.named_scope("fwdq"):
         @pl.loop(0, half)
@@ -335,7 +350,7 @@
     def widest(i):
         h = lax.div(i, 2)
 
-        @pl.when(after[3])
+        @pl.when(before[1] & after[3])
         def _():
             send_q3(i).wait_recv()
             for s in range(2):
@@ -350,6 +365,22 @@
                 o3[t] = (o * (1.0 / total)).astype(BF16)
                 l3[t] = top + jnp.log2(total)
             for copy in send_o3(i):
+                copy.start()
+
+    def extra(i):
+        h = lax.div(i, 2)
+
+        @pl.when((c == 1) & after[2])
+        def _():
+            send_qx(i).wait_recv()
+            for s in range(2):
+                t = 2 * i + s
+                g = t - h * G
+                top, total, (p3,) = softmax_of([scores_of(rows_of(k1, h, g), rows_of(qx, t), bias2[...])])
+                o = jnp.dot(v1t[h, :, tile(g)], p3, preferred_element_type=F32)
+                ox[t] = (o * (1.0 / total)).astype(BF16)
+                lx[t] = top + jnp.log2(total)
+            for copy in send_ox(i):
                 copy.start()
 
     def local(h):
@@ -394,6 +425,7 @@
             context(h)
             for s in range(2):
                 widest(2 * h + s)
+                extra(2 * h + s)
 
     with jax.named_scope("local01_fwd"):
         @pl.loop(0, heads // 2)
@@ -413,6 +445,7 @@
         def _(i):
             answer(i)
             widest(half + i)
+            extra(half + i)
 
     def row_block(b):
         return slice(b * T, (b + 1) * T)
@@ -444,10 +477,10 @@
             for b in range(G):
                 y = term(tp, h, b)
                 acc[row_block(b)] = y if h == 0 else acc[row_block(b)] + y
-            if h > 0:
-                send_mixed(h - 1).wait_recv()
+            if h < heads - 1:
+                send_mixed(h).wait_recv()
                 for b in range(G):
-                    acc[row_block(b)] += term(1 - tp, h - 1, b)
+                    acc[row_block(b)] += term(1 - tp, h, b)
 
     load(4).wait()
     with jax.named_scope("final"):
@@ -486,11 +519,20 @@
             def _():
                 send_q1(i).wait_send()
 
-            @pl.when(before[2] & after[1])
+            @pl.when(before[3] & after[1])
             def _():
                 send_q3(i).wait_send()
 
-            @pl.when(after[3])
+            @pl.when((c == 2) & after[1])
+            def _():
+                send_qx(i).wait_send()
+
+            @pl.when((c == 1) & after[2])
+            def _():
+                for copy in send_ox(i):
+                    copy.wait_send()
+
+            @pl.when(before[1] & after[3])
             def _():
                 for copy in send_o3(i):
                     copy.wait_send()
@@ -532,13 +574,13 @@
         vmem(split, BF16),
         vmem(by_head, BF16), vmem(by_head, BF16), vmem(by_head, BF16), vmem(by_head, BF16),
         vmem(turned, BF16), vmem(turned, BF16),
-        vmem(split, BF16), vmem(split, BF16),
+        vmem(split, BF16), vmem(split, BF16), vmem(split, BF16), vmem(square, BF16), vmem(stat, F32),
         vmem(square, BF16), vmem(stat, F32), vmem(square, BF16), vmem(stat, F32),
         vmem(square, BF16), vmem(stat, F32), vmem(square, BF16), vmem(stat, F32),
         vmem(square, F32), vmem(stat, F32), vmem(stat, F32),
         vmem(turned, BF16), vmem((2, heads, ROWS, HEAD), BF16),
         dma((5,)), dma((2, 1)), dma((2, chunks)), dma((2, chunks)), dma((2, chunks)), dma((2, chunks)),
-        dma((2, chunks)), dma((2, chunks)), dma((2, chunks)), dma((2, chunks)), dma((2, heads)), dma((G,)),
+        dma((2, chunks)), dma((2, chunks)), dma((2, chunks)), dma((2, chunks)), dma((2, chunks)), dma((2, chunks)), dma((2, heads)), dma((G,)),
     ]
     hbm = pl.BlockSpec(memory_space=pltpu.HBM)
     return pl.pallas_call(

time: 84.9 us -> 76.2 us (0.90)
  Pallas kernels: 83.9 us -> 75.1 us
    pallas_call x1, Pallas kernels: 83.9 us -> 75.1 us  [body(): pl.pallas_call(functools.partial(kernel, n), out_shape=jax.ShapeDtypeStru...]
where the time goes in v4:
time: 76.2 us; the launch traced here: 76.1 us
  Pallas kernels  75.1 us (99%)
  local copies, waits for them, and re-layouts  0.97 us (1%)
    pallas_call x1, Pallas kernels, body(): pl.pallas_call(functools.partial(kernel, n), out_shape=jax.ShapeDtypeStru...  75.1 us

profile of v4, /device:TPU:293, one launch (start us, length us, event | category | flops | bytes accessed | tf_op | source)
XLA Modules:
  0.0 76.1 jit_solution(13488292901422579645)
XLA Ops:
  0.0 75.1 %attention.1 = bf16[512,1024]{1,0:T(8,128)(2,1)S(1)} custom-call(bf16[256,2048]{1,0:T(8,128)(2,1)} %tokens.1, bf16[2048,512]{1,0:T(8,128)(2,1)} %wq.1, bf16[2048,512]{1,0:T(8,128)(2,1)} %wk.1, bf16[2048,512]{1,0:T(8,128)(2,1)} %wv.1, bf16[1024,1024]{1,0:T(8,128)(2,1)} %wo.1), custom_call_target="tpu_custom_call" | custom-call | tf_op jit(solution)/shard_map/attention/pallas_call | solution.py:586
  75.1 1.0 %copy.7 = bf16[512,1024]{1,0:T(8,128)(2,1)} copy(bf16[512,1024]{1,0:T(8,128)(2,1)S(1)} %attention.1) | data formatting | bytes 2097152

commit v5 on v4

--- a/solution.py
+++ b/solution.py
@@ -419,33 +419,42 @@
             for copy in send_o1(i):
                 copy.start()
 
-    with jax.named_scope("ctx01_o3"):
-        @pl.loop(0, heads // 2)
-        def _(h):
-            context(h)
-            for s in range(2):
-                widest(2 * h + s)
-                extra(2 * h + s)
-
-    with jax.named_scope("local01_fwd"):
-        @pl.loop(0, heads // 2)
-        def _(h):
-            local(h)
-            for s in range(2):
-                pass_on(half + 2 * h + s)
-
-    with jax.named_scope("ctx23_local"):
-        @pl.loop(heads // 2, heads)
-        def _(h):
-            context(h)
-            local(h)
-
-    with jax.named_scope("o1_o3"):
-        @pl.loop(0, half)
-        def _(i):
-            answer(i)
-            widest(half + i)
-            extra(half + i)
+    def i32(i):
+        return jnp.int32(i)
+
+    def wide(i):
+        widest(i32(i))
+        extra(i32(i))
+
+    with jax.named_scope("wide03"):
+        context(0)
+        wide(0)
+        wide(1)
+        context(1)
+        wide(2)
+        pass_on(half)
+        wide(3)
+        pass_on(half + 1)
+    with jax.named_scope("local0"):
+        local(0)
+        pass_on(half + 2)
+        answer(i32(0))
+    with jax.named_scope("local1"):
+        local(1)
+        pass_on(half + 3)
+        answer(i32(1))
+        answer(i32(2))
+    with jax.named_scope("wide45"):
+        context(2)
+        wide(4)
+        answer(i32(3))
+        local(2)
+        wide(5)
+    with jax.named_scope("wide67"):
+        context(3)
+        wide(6)
+        local(3)
+        wide(7)
 
     def row_block(b):
         return slice(b * T, (b + 1) * T)

time: 76.2 us -> 72.4 us (0.950)
  Pallas kernels: 75.1 us -> 71.3 us
    pallas_call x1, Pallas kernels: 75.1 us -> 71.3 us  [body(): pl.pallas_call(functools.partial(kernel, n), out_shape=jax.ShapeDtypeStru...]
where the time goes in v5:
time: 72.4 us; the launch traced here: 72.3 us
  Pallas kernels  71.3 us (98%)
  local copies, waits for them, and re-layouts  0.97 us (1%)
    pallas_call x1, Pallas kernels, body(): pl.pallas_call(functools.partial(kernel, n), out_shape=jax.ShapeDtypeStru...  71.3 us

profile of v5, /device:TPU:293, one launch (start us, length us, event | category | flops | bytes accessed | tf_op | source)
XLA Modules:
  0.0 72.3 jit_solution(11655526225636227820)
XLA Ops:
  0.0 71.3 %attention.1 = bf16[512,1024]{1,0:T(8,128)(2,1)S(1)} custom-call(bf16[256,2048]{1,0:T(8,128)(2,1)} %tokens.1, bf16[2048,512]{1,0:T(8,128)(2,1)} %wq.1, bf16[2048,512]{1,0:T(8,128)(2,1)} %wk.1, bf16[2048,512]{1,0:T(8,128)(2,1)} %wv.1, bf16[1024,1024]{1,0:T(8,128)(2,1)} %wo.1), custom_call_target="tpu_custom_call" | custom-call | tf_op jit(solution)/shard_map/attention/pallas_call | solution.py:595
  71.3 1.0 %copy.7 = bf16[512,1024]{1,0:T(8,128)(2,1)} copy(bf16[512,1024]{1,0:T(8,128)(2,1)S(1)} %attention.1) | data formatting | bytes 2097152

commit v6 on v5

--- a/solution.py
+++ b/solution.py
@@ -183,11 +183,10 @@
             for g in range(G):
                 v0[2 * p + s, g, u] = y[g * piece:(g + 1) * piece, s * HEAD:(s + 1) * HEAD]
 
-    def forward(send, p, u):
+    def forward(send, h, u):
         @pl.when(after[1])
         def _():
-            for s in range(2):
-                send(2 * p + s, u).start()
+            send(h, u).start()
 
     with jax.named_scope("own_k"):
         load(0).wait()
@@ -248,7 +247,9 @@
         forward(send_k, 0, 1 - tp)
         make_v(0, 1 - tp)
         forward(send_v, 0, 1 - tp)
-        forward(send_k, 1, tp)
+        for u in (tp, 1 - tp):
+            forward(send_k, 1, u)
+            forward(send_v, 1, u)
 
     with jax.named_scope("q0"):
         load(3).wait()
@@ -257,11 +258,12 @@
 
     with jax.named_scope("kv1"):
         make_v(1, tp)
-        forward(send_v, 1, tp)
         make_k(1, 1 - tp)
-        forward(send_k, 1, 1 - tp)
         make_v(1, 1 - tp)
-        forward(send_v, 1, 1 - tp)
+        for h in (2, 3):
+            for u in (tp, 1 - tp):
+                forward(send_k, h, u)
+                forward(send_v, h, u)
 
     with jax.named_scope("q1"):
         make_q(1)
@@ -426,24 +428,33 @@
         widest(i32(i))
         extra(i32(i))
 
+    def early(i):
+        pl.when(after[2])(functools.partial(pass_on, i))
+
     with jax.named_scope("wide03"):
         context(0)
         wide(0)
         wide(1)
         context(1)
         wide(2)
-        pass_on(half)
+        early(half)
         wide(3)
-        pass_on(half + 1)
+        early(half + 1)
     with jax.named_scope("local0"):
         local(0)
-        pass_on(half + 2)
+        early(half + 2)
         answer(i32(0))
     with jax.named_scope("local1"):
         local(1)
-        pass_on(half + 3)
+        early(half + 3)
         answer(i32(1))
         answer(i32(2))
+
+        @pl.when(c + 2 == n)
+        def _():
+            for i in range(half, chunks):
+                pass_on(i)
+
     with jax.named_scope("wide45"):
         context(2)
         wide(4)

time: 72.4 us -> 70.6 us (0.975)
  Pallas kernels: 71.3 us -> 69.5 us
    pallas_call x1, Pallas kernels: 71.3 us -> 69.5 us  [body(): pl.pallas_call(functools.partial(kernel, n), out_shape=jax.ShapeDtypeStru...]
where the time goes in v6:
time: 70.6 us; the launch traced here: 70.5 us
  Pallas kernels  69.5 us (98%)
  local copies, waits for them, and re-layouts  0.97 us (1%)
    pallas_call x1, Pallas kernels, body(): pl.pallas_call(functools.partial(kernel, n), out_shape=jax.ShapeDtypeStru...  69.5 us

profile of v6, /device:TPU:293, one launch (start us, length us, event | category | flops | bytes accessed | tf_op | source)
XLA Modules:
  0.0 70.5 jit_solution(4060938624605637642)
XLA Ops:
  0.0 69.5 %attention.1 = bf16[512,1024]{1,0:T(8,128)(2,1)S(1)} custom-call(bf16[256,2048]{1,0:T(8,128)(2,1)} %tokens.1, bf16[2048,512]{1,0:T(8,128)(2,1)} %wq.1, bf16[2048,512]{1,0:T(8,128)(2,1)} %wk.1, bf16[2048,512]{1,0:T(8,128)(2,1)} %wv.1, bf16[1024,1024]{1,0:T(8,128)(2,1)} %wo.1), custom_call_target="tpu_custom_call" | custom-call | tf_op jit(solution)/shard_map/attention/pallas_call | solution.py:606
  69.5 1.0 %copy.7 = bf16[512,1024]{1,0:T(8,128)(2,1)} copy(bf16[512,1024]{1,0:T(8,128)(2,1)S(1)} %attention.1) | data formatting | bytes 2097152

commit v7 on v6

--- a/solution.py
+++ b/solution.py
@@ -73,7 +73,7 @@
         src, dst = ((tokens, x_nat.at[tp]), (wk, wk_v), (wv, wv_v), (wq, wq_v), (wo, wo_v))[i]
         return pltpu.make_async_copy(src, dst, load_sem.at[i])
 
-    for i in range(5):
+    for i in range(2):
         load(i).start()
 
     barrier = pltpu.get_barrier_semaphore()
@@ -190,8 +190,11 @@
 
     with jax.named_scope("own_k"):
         load(0).wait()
+        load(2).start()
         permuted(tp)
         load(1).wait()
+        for i in (3, 4):
+            load(i).start()
         make_k(0, tp)
 
     with jax.named_scope("barrier"):

time: 70.6 us -> 70.6 us (level)
  no operation moved by 1% of the time
where the time goes in v7:
time: 70.6 us; the launch traced here: 70.5 us
  Pallas kernels  69.6 us (99%)
  local copies, waits for them, and re-layouts  0.97 us (1%)
    pallas_call x1, Pallas kernels, body(): pl.pallas_call(functools.partial(kernel, n), out_shape=jax.ShapeDtypeStru...  69.6 us

profile of v7, /device:TPU:293, one launch (start us, length us, event | category | flops | bytes accessed | tf_op | source)
XLA Modules:
  0.0 70.5 jit_solution(17709321233475963205)
XLA Ops:
  0.0 69.6 %attention.1 = bf16[512,1024]{1,0:T(8,128)(2,1)S(1)} custom-call(bf16[256,2048]{1,0:T(8,128)(2,1)} %tokens.1, bf16[2048,512]{1,0:T(8,128)(2,1)} %wq.1, bf16[2048,512]{1,0:T(8,128)(2,1)} %wk.1, bf16[2048,512]{1,0:T(8,128)(2,1)} %wv.1, bf16[1024,1024]{1,0:T(8,128)(2,1)} %wo.1), custom_call_target="tpu_custom_call" | custom-call | tf_op jit(solution)/shard_map/attention/pallas_call | solution.py:609
  69.6 1.0 %copy.7 = bf16[512,1024]{1,0:T(8,128)(2,1)} copy(bf16[512,1024]{1,0:T(8,128)(2,1)S(1)} %attention.1) | data formatting | bytes 2097152
